TPU v7x, 512 devices: a whole 4x4x16 slice. The times are simulated.
512 devices in a mesh: rep: 2 (over z_hi), fs: 32 (over z_lo, y), tp: 8 (over x, core).
Axes of the slice: x: 4, y: 4, z: 16 (z_hi: 2, z_lo: 8; z = z_hi * 8 + z_lo), core: 2. Of those that a mesh axis runs over, the one named last changes fastest.
Arguments:
- tokens: bfloat16 [64, 1024, 1024], P(('rep', 'fs'), 'tp'), may hold values from -6 to 6
- mixer_in_gain: float32 [1024], replicated, may hold values from 0.5 to 1.5
- query_weight: bfloat16 [1024, 1024], P('fs', 'tp'), may hold values from -0.1875 to 0.1875
- key_weight: bfloat16 [1024, 1024], P('fs', 'tp'), may hold values from -0.1875 to 0.1875
- value_weight: bfloat16 [1024, 2048], P('fs', 'tp'), may hold values from -0.1875 to 0.1875
- gate_weight: bfloat16 [1024, 2048], P('fs', 'tp'), may hold values from -0.1875 to 0.1875
- decay_logits: float32 [2, 8], P(None, 'tp'), may hold values from 3.4 to 6.2
- mixer_output: bfloat16 [2048, 1024], P('tp', 'fs'), may hold values from -0.125 to 0.125
- mixer_out_gain: float32 [1024], replicated, may hold values from 0.5 to 1.5
- channel_in_gain: float32 [1024], replicated, may hold values from 0.5 to 1.5
- gelu_weight: bfloat16 [1024, 2816], P('fs', 'tp'), may hold values from -0.1875 to 0.1875
- linear_weight: bfloat16 [1024, 2816], P('fs', 'tp'), may hold values from -0.1875 to 0.1875
- gelu_kernel: float32 [3, 2816], P(None, 'tp'), may hold values from -3.5 to 3.5
- linear_kernel: float32 [3, 2816], P(None, 'tp'), may hold values from -3.5 to 3.5
- gelu_bias: float32 [2816], P('tp'), may hold values from -1.2 to 1.2
- linear_bias: float32 [2816], P('tp'), may hold values from -1.2 to 1.2
- down_weight: bfloat16 [2816, 1024], P('tp', 'fs'), may hold values from -0.109375 to 0.109375
- channel_out_gain: float32 [1024], replicated, may hold values from 0.5 to 1.5
Outputs:
- layer_output: bfloat16 [64, 1024, 1024], P(('rep', 'fs'), 'tp')
All inputs are finite; a program needn't handle non-finite values.
Results may differ from a plain program's by a relative error of at most 0.02.
Values may be sent and summed in bfloat16 or wider, within the bound.
A program may use at most 64 MiB of HBM per device.

v0:
```python
import jax
import jax.numpy as jnp
from jax import lax
from jax.sharding import Mesh
from jax.sharding import PartitionSpec as P

DK = 128
DV = 256
SPAN = 128
TP = ("tp_0", "tp_1")


epsilon = 1e-06
rope_base = 10000.0


def joined_along(pieces, dim):
    lengths = list(pieces.shape[1:])
    lengths[dim] *= pieces.shape[0]
    return jnp.moveaxis(pieces, 0, dim).reshape(lengths)


def gather_together(arrays, axis, dims):
    flat = jnp.concatenate([a.reshape(-1) for a in arrays])
    lines, at, gathered = lax.all_gather(flat, axis), 0, []
    for a, dim in zip(arrays, dims):
        pieces = lines[:, at : at + a.size].reshape(-1, *a.shape)
        gathered.append(joined_along(pieces, dim))
        at += a.size
    return tuple(gathered)


def piece_ends(length, count):
    unit = 8 if length >= 8 * count else 1
    return [length // unit * k // count * unit for k in range(1, count)]


def all_blocks(value, axes, order):
    pieces = value[None]
    for k in order:
        pieces = lax.all_gather(pieces, axes[k], axis=0, tiled=True)
    carried = [lax.axis_size(axes[k]) for k in reversed(order)]
    pieces = pieces.reshape(*carried, *value.shape)
    turned = sorted(range(len(order)), key=lambda place: order[len(order) - 1 - place])
    return pieces.transpose(*turned, *range(len(order), pieces.ndim)).reshape(-1, *value.shape)


def gather_at_once(value, axes, dim):
    cut = max(range(max(1, value.ndim - 1)), key=lambda d: value.shape[d])
    count, gathered = len(axes), []
    for leading, piece in enumerate(
        jnp.split(value, piece_ends(value.shape[cut], count), axis=cut)
    ):
        if piece.size:
            order = [(leading - k) % count for k in range(count)]
            gathered.append(all_blocks(piece, axes, order))
    return joined_along(jnp.concatenate(gathered, axis=cut + 1), dim)


def on_whole(value, axes, dim, work):
    everything = gather_at_once(value, axes, dim)
    return work(everything, jnp.int32(0))


def own_rows_2(product, extent, axis):
    everything = product(jnp.int32(0), lax.axis_size(axis) * extent)
    own = lax.psum_scatter(everything.astype(jnp.bfloat16), axis, scatter_dimension=0, tiled=True)
    return own.astype(jnp.float32)


def rms_scaled(row_values, norm_gain):
    values = row_values.astype(jnp.float32)
    return (
        values * lax.rsqrt(jnp.mean(values * values, axis=-1, keepdims=True) + epsilon) * norm_gain
    )


def rotate(values, positions):
    half_width = values.shape[-1] // 2
    frequency = 1.0 / rope_base ** (jnp.arange(half_width, dtype=jnp.float32) / half_width)
    angles = positions.astype(jnp.float32)[:, None] * frequency[None, :]
    cosine = jnp.cos(angles)[:, None, :]
    sine_part = jnp.sin(angles)[:, None, :]
    first_half = values[..., :half_width]
    second = values[..., half_width:]
    return jnp.concatenate(
        [first_half * cosine - second * sine_part, first_half * sine_part + second * cosine],
        axis=-1,
    )


def one_direction(queries, key_rows, value_rows, log_decay, strict):
    highest = lax.Precision.HIGHEST
    length = queries.shape[0]
    head_count = queries.shape[1]
    block_count = length // SPAN
    inside_index = jnp.arange(SPAN, dtype=jnp.float32)
    offset = inside_index[:, None] - inside_index[None, :]
    allowed = offset >= (1.0 if strict else 0.0)
    within = jnp.where(
        allowed[None],
        jnp.exp(jnp.where(allowed, offset, 0.0)[None] * log_decay[:, None, None]),
        0.0,
    )
    query_blocks = queries.reshape(block_count, SPAN, head_count, -1)
    key_blocks = key_rows.reshape(block_count, SPAN, head_count, -1)
    value_blocks = value_rows.reshape(block_count, SPAN, head_count, -1).astype(jnp.float32)
    scores = (
        jnp.einsum("nchd,nmhd->nhcm", query_blocks, key_blocks, preferred_element_type=jnp.float32)
        * within[None]
    )
    inside = jnp.einsum("nhcm,nmhe->nche", scores, value_blocks, precision=highest)
    tail_decay = jnp.exp((SPAN - 1.0 - inside_index)[:, None] * log_decay[None, :])
    lead_decay = jnp.exp((inside_index + 1.0)[:, None] * log_decay[None, :])
    step_decay = jnp.exp(SPAN * log_decay)
    updates = jnp.einsum(
        "nmhd,nmhe->nhde",
        key_blocks.astype(jnp.float32),
        value_blocks * tail_decay[None, :, :, None],
        precision=highest,
    )

    def advance(carried, update):
        return (step_decay[:, None, None] * carried + update, carried)

    _, before = lax.scan(advance, jnp.zeros(updates.shape[1:], jnp.float32), updates)
    across = jnp.einsum(
        "nchd,nhde->nche",
        query_blocks.astype(jnp.float32) * lead_decay[None, :, :, None],
        before,
        precision=highest,
    )
    return (inside + across).reshape(length, head_count, -1)


def retention(queries, key_rows, value_rows, logits):
    log_forward = jax.nn.log_sigmoid(logits[0])
    log_backward = jax.nn.log_sigmoid(logits[1])
    forward = one_direction(queries, key_rows, value_rows, log_forward, False)
    behind = one_direction(queries[::-1], key_rows[::-1], value_rows[::-1], log_backward, True)[
        ::-1
    ]
    return forward + behind


def head_norm(values):
    centred = values - jnp.mean(values, axis=-1, keepdims=True)
    return centred * lax.rsqrt(jnp.mean(centred * centred, axis=-1, keepdims=True) + epsilon)


def conv_positions(values, kernel, biases):
    padded = jnp.pad(values.astype(jnp.float32), ((1, 1), (0, 0)))
    return kernel[0] * padded[:-2] + kernel[1] * padded[1:-1] + kernel[2] * padded[2:] + biases


def per_device(
    tokens,
    mixer_in_gain,
    query_weight,
    key_weight,
    value_weight,
    gate_weight,
    decay_logits,
    mixer_output,
    mixer_out_gain,
    channel_in_gain,
    gelu_weight,
    linear_weight,
    gelu_kernel,
    linear_kernel,
    gelu_bias,
    linear_bias,
    down_weight,
    channel_out_gain,
):
    token_rows = tokens[0]
    own_rows = token_rows.shape[0]
    normed = rms_scaled(token_rows, mixer_in_gain).astype(jnp.bfloat16)
    query_full, key_full, value_full, gate_full = gather_together(
        (query_weight, key_weight, value_weight, gate_weight), "fs", (0, 0, 0, 0)
    )
    query_width = query_full.shape[1]
    value_width = value_full.shape[1]
    head_count = query_width // DK

    def project(row_block, first_row):
        row_total = row_block.shape[0]
        positions = first_row + jnp.arange(row_total, dtype=jnp.int32)
        query_raw = jnp.dot(row_block, query_full, preferred_element_type=jnp.float32).reshape(
            row_total, head_count, DK
        )
        query_part = rotate(query_raw, positions).reshape(row_total, query_width)
        key_raw = jnp.dot(row_block, key_full, preferred_element_type=jnp.float32).reshape(
            row_total, head_count, DK
        )
        key_part = (rotate(key_raw, positions) * DK ** (-0.5)).reshape(row_total, query_width)
        value_part = jnp.dot(row_block, value_full, preferred_element_type=jnp.float32)
        gate_part = jnp.dot(row_block, gate_full, preferred_element_type=jnp.float32)
        return jnp.concatenate([query_part, key_part, value_part, gate_part], axis=1).astype(
            jnp.bfloat16
        )

    joined = on_whole(normed, TP, 0, project)
    length = joined.shape[0]
    queries = joined[:, :query_width].reshape(length, head_count, DK)
    key_rows = joined[:, query_width : 2 * query_width].reshape(length, head_count, DK)
    value_rows = joined[:, 2 * query_width : 2 * query_width + value_width].reshape(
        length, head_count, DV
    )
    gate_rows = joined[:, 2 * query_width + value_width :]
    retained = retention(queries, key_rows, value_rows, decay_logits)
    gated = (
        head_norm(retained).reshape(length, value_width)
        * jax.nn.silu(gate_rows.astype(jnp.float32))
    ).astype(jnp.bfloat16)
    output_columns = lax.all_gather(mixer_output, "fs", axis=1, tiled=True)

    def mixer_term(first_row, row_count):
        row_part = lax.dynamic_slice_in_dim(gated, first_row, row_count, 0)
        return jnp.dot(row_part, output_columns, preferred_element_type=jnp.float32)

    mix_sum = own_rows_2(mixer_term, own_rows, TP)
    after_mix = (token_rows.astype(jnp.float32) + rms_scaled(mix_sum, mixer_out_gain)).astype(
        jnp.bfloat16
    )
    channel_in = rms_scaled(after_mix, channel_in_gain).astype(jnp.bfloat16)
    gelu_full, linear_full = gather_together((gelu_weight, linear_weight), "fs", (0, 0))

    def expand(row_block, first_row):
        gelu_part = jnp.dot(row_block, gelu_full, preferred_element_type=jnp.float32)
        linear_part = jnp.dot(row_block, linear_full, preferred_element_type=jnp.float32)
        return jnp.concatenate([gelu_part, linear_part], axis=1).astype(jnp.bfloat16)

    both_parts = on_whole(channel_in, TP, 0, expand)
    gelu_in = both_parts[:, : gelu_full.shape[1]]
    linear_in = both_parts[:, gelu_full.shape[1] :]
    hidden = (
        jax.nn.gelu(conv_positions(gelu_in, gelu_kernel, gelu_bias))
        * conv_positions(linear_in, linear_kernel, linear_bias)
    ).astype(jnp.bfloat16)
    down_columns = lax.all_gather(down_weight, "fs", axis=1, tiled=True)

    def channel_term(first_row, row_count):
        row_part = lax.dynamic_slice_in_dim(hidden, first_row, row_count, 0)
        return jnp.dot(row_part, down_columns, preferred_element_type=jnp.float32)

    channel_sum = own_rows_2(channel_term, own_rows, TP)
    result = (after_mix.astype(jnp.float32) + rms_scaled(channel_sum, channel_out_gain)).astype(
        jnp.bfloat16
    )
    return result[None]


def solution(mesh):
    split = Mesh(
        mesh.devices.reshape(mesh.shape["rep"], mesh.shape["fs"], 4, 2),
        ("rep", "fs", "tp_0", "tp_1"),
    )
    in_specs = (
        P(("rep", "fs"), TP, None),
        P(),
        P("fs", TP),
        P("fs", TP),
        P("fs", TP),
        P("fs", TP),
        P(None, TP),
        P(TP, "fs"),
        P(),
        P(),
        P("fs", TP),
        P("fs", TP),
        P(None, TP),
        P(None, TP),
        P(TP),
        P(TP),
        P(TP, "fs"),
        P(),
    )
    out_specs = P(("rep", "fs"), TP, None)
    return jax.shard_map(
        per_device, mesh=split, in_specs=in_specs, out_specs=out_specs, check_vma=False
    )
```

profile of v0, /device:TPU:1, one launch (start us, length us, event | category | flops | bytes accessed | tf_op | source)
XLA Modules:
  0.0 769.6 jit_solution(12787065556506595714)
XLA Ops:
  8.8 12.3 %all-gather = bf16[256,1024]{1,0:T(8,128)(2,1)} all-gather(bf16[64,1024]{1,0:T(8,128)(2,1)S(1)} %get-tuple-element.171), channel_id=2, replica_groups=mesh['rep'=2,'fs'=32,'tp_0'=4,'tp_1'=2] {'tp_0'}, dimensions={0}, use_global_device_ids=true | all-gather | bytes 655360 | tf_op jit(solution)/shard_map/all_gather | solution.py:41
  21.2 10.0 %all-gather.1 = bf16[128,1024]{1,0:T(8,128)(2,1)} all-gather(bf16[64,1024]{1,0:T(8,128)(2,1)S(1)} %get-tuple-element.172), channel_id=3, replica_groups=mesh['rep'=2,'fs'=32,'tp_0'=4,'tp_1'=2] {'tp_1'}, dimensions={0}, use_global_device_ids=true | all-gather | bytes 393216 | tf_op jit(solution)/shard_map/all_gather | solution.py:41
  35.0 113.6 %all_gather.48 = bf16[256,1024]{0,1:T(8,128)(2,1)} all-gather(bf16[256,32]{0,1:T(8,128)(2,1)S(1)} %copy-done.15), channel_id=1, replica_groups=mesh['rep'=2,'fs'=32,'tp_0'=4,'tp_1'=2] {'fs'}, dimensions={1}, use_global_device_ids=true | all-gather | bytes 540672 | tf_op jit(solution)/shard_map/all_gather | solution.py:216
  151.5 133.9 %all-gather.21.cloned.1.call-done = bf16[786432]{0:T(1024)(128)(2,1)} async-done(((bf16[24576]{0:T(1024)(128)(2,1)}), bf16[786432]{0:T(1024)(128)(2,1)}) %all-gather.21.cloned.1.call-update) | async-done | bytes 1572880 | tf_op jit(solution)/shard_map/all_gather | solution.py:25
  285.4 2.7 reshape.445
  289.1 2.1 fusion.99
  292.2 1.8 convolution_bitcast_fusion.2
  294.8 1.9 fusion.71
  301.7 1.8 fusion.48
  306.4 1.8 convolution_bitcast_fusion.1
  309.3 13.0 %while.26 = (s32[]{:T(128)}, f32[1,128,256]{2,1,0:T(8,128)S(1)}, f32[8,1,128,256]{3,2,1,0:T(8,128)}, f32[1]{0:T(128)}, f32[8,1,128,256]{3,2,1,0:T(8,128)}, /*index=5*/s32[]{:T(128)}, s32[]{:T(128)}) while((s32[]{:T(128)}, f32[1,128,256]{2,1,0:T(8,128)S(1)}, f32[8,1,128,256]{3,2,1,0:T(8,128)}, f32[1]{0:T(128)}, ...), condition=%wide.region_2.3_spmd.clone, body=%wide.region_1.2_spmd.clone.sunk | while | flops 131075 | bytes 655968 | solution.py:126
  322.3 3.5 reverse.11
  325.9 2.9 reverse.10
  331.7 1.8 convolution_bitcast_fusion
  334.6 13.0 %while.27 = (s32[]{:T(128)}, f32[1,128,256]{2,1,0:T(8,128)S(1)}, f32[8,1,128,256]{3,2,1,0:T(8,128)}, f32[1]{0:T(128)}, f32[8,1,128,256]{3,2,1,0:T(8,128)}, /*index=5*/s32[]{:T(128)}, s32[]{:T(128)}) while((s32[]{:T(128)}, f32[1,128,256]{2,1,0:T(8,128)S(1)}, f32[8,1,128,256]{3,2,1,0:T(8,128)}, f32[1]{0:T(128)}, ...), condition=%wide.region_4.5_spmd.clone, body=%wide.region_3.4_spmd.clone.sunk | while | flops 131075 | bytes 655968 | solution.py:126
  347.6 3.3 convolution_add_fusion
  350.9 9.0 %rev.2 = f32[1024,1,256]{2,0,1:T(8,128)} reverse(f32[1024,1,256]{2,0,1:T(8,128)} %bitcast.150), dimensions={0} | reverse | bytes 2097152 | tf_op jit(solution)/shard_map/rev | solution.py:140
  359.9 2.4 convolution_add_fusion.1
  363.0 2.1 reshape_reshape.24
  365.1 4.7 convolution_convert_fusion.1
  371.5 59.3 %reduce-scatter.3.cloned.1.call-done = bf16[128,1024]{1,0:T(8,128)(2,1)} async-done(((bf16[1024,1024]{1,0:T(8,128)(2,1)}), bf16[128,1024]{1,0:T(8,128)(2,1)}) %reduce-scatter.3.cloned.1.call-update) | async-done | bytes 262160 | tf_op jit(solution)/shard_map/reduce_scatter | solution.py:67
  433.3 12.0 %all-gather.3 = bf16[256,1024]{1,0:T(8,128)(2,1)} all-gather(bf16[64,1024]{1,0:T(8,128)(2,1)S(1)} %get-tuple-element.167), channel_id=5, replica_groups=mesh['rep'=2,'fs'=32,'tp_0'=4,'tp_1'=2] {'tp_0'}, dimensions={0}, use_global_device_ids=true | all-gather | bytes 655360 | tf_op jit(solution)/shard_map/all_gather | solution.py:41
  445.5 117.5 %all_gather.55 = bf16[352,1024]{0,1:T(8,128)(2,1)} all-gather(bf16[352,32]{0,1:T(8,128)(2,1)S(1)} %copy-done.12), channel_id=1, replica_groups=mesh['rep'=2,'fs'=32,'tp_0'=4,'tp_1'=2] {'fs'}, dimensions={1}, use_global_device_ids=true | all-gather | bytes 743424 | tf_op jit(solution)/shard_map/all_gather | solution.py:241
  563.0 70.6 %all-gather.23.cloned.1.call-done = bf16[720896]{0:T(1024)(128)(2,1)} async-done(((bf16[22528]{0:T(1024)(128)(2,1)}), bf16[720896]{0:T(1024)(128)(2,1)}) %all-gather.23.cloned.1.call-update) | async-done | bytes 1441808 | tf_op jit(solution)/shard_map/all_gather | solution.py:25
  635.3 25.1 %all-gather.4 = bf16[128,1024]{1,0:T(8,128)(2,1)} all-gather(bf16[64,1024]{1,0:T(8,128)(2,1)S(1)} %get-tuple-element.168), channel_id=6, replica_groups=mesh['rep'=2,'fs'=32,'tp_0'=4,'tp_1'=2] {'tp_1'}, dimensions={0}, use_global_device_ids=true | all-gather | bytes 393216 | tf_op jit(solution)/shard_map/all_gather | solution.py:41
  660.6 2.1 reshape_reshape.26
  662.6 2.1 reshape_reshape.25
  664.7 12.2 %all-gather.17.cloned.1.call-done = bf16[8,64,1024]{2,1,0:T(8,128)(2,1)} async-done(((bf16[4,64,1024]{2,1,0:T(8,128)(2,1)}), bf16[8,64,1024]{2,1,0:T(8,128)(2,1)}) %all-gather.17.cloned.1.call-update) | async-done | bytes 1048592 | tf_op jit(solution)/shard_map/all_gather | solution.py:41
  678.2 30.1 %all-gather.19.cloned.1.call-done = bf16[8,64,1024]{2,1,0:T(8,128)(2,1)} async-done(((bf16[2,64,1024]{2,1,0:T(8,128)(2,1)}), bf16[8,64,1024]{2,1,0:T(8,128)(2,1)}) %all-gather.19.cloned.1.call-update) | async-done | bytes 1048592 | tf_op jit(solution)/shard_map/all_gather | solution.py:41
  712.2 4.8 convolution_convert_fusion
  717.0 42.9 %reduce-scatter.5.cloned.1.call-done = bf16[128,1024]{1,0:T(8,128)(2,1)} async-done(((bf16[1024,1024]{1,0:T(8,128)(2,1)}), bf16[128,1024]{1,0:T(8,128)(2,1)}) %reduce-scatter.5.cloned.1.call-update) | async-done | bytes 262160 | tf_op jit(solution)/shard_map/reduce_scatter | solution.py:67
  761.0 1.8 fusion.74
  (162 shorter events, 61.8 us)
Async XLA Ops:
  6.5 142.1 %all-gather.13.cloned.1.call-start = ((), (), s32[]{:S(2)}) async-start(), calls=%async_computation.2 | async-start | bytes 1572864 | tf_op jit(solution)/shard_map/all_gather | solution.py:41
  7.6 23.6 %copy-start.16 = (bf16[32,256]{1,0:T(8,128)(2,1)S(1)}, bf16[32,256]{1,0:T(8,128)(2,1)}, u32[]{:S(2)}) copy-start(bf16[32,256]{1,0:T(8,128)(2,1)} %param.26) | copy-start | bytes 49156
  7.6 23.6 %copy-start.17 = (bf16[32,256]{1,0:T(8,128)(2,1)S(1)}, bf16[32,256]{1,0:T(8,128)(2,1)}, u32[]{:S(2)}) copy-start(bf16[32,256]{1,0:T(8,128)(2,1)} %param.27) | copy-start | bytes 49156
  7.7 23.7 %copy-start.18 = (bf16[32,128]{1,0:T(8,128)(2,1)S(1)}, bf16[32,128]{1,0:T(8,128)(2,1)}, u32[]{:S(2)}) copy-start(bf16[32,128]{1,0:T(8,128)(2,1)} %param.25) | copy-start | bytes 24580
  7.7 23.7 %copy-start.19 = (bf16[32,128]{1,0:T(8,128)(2,1)S(1)}, bf16[32,128]{1,0:T(8,128)(2,1)}, u32[]{:S(2)}) copy-start(bf16[32,128]{1,0:T(8,128)(2,1)} %param.24) | copy-start | bytes 24580
  7.7 24.4 %copy-start.25 = (f32[2,1]{0,1:T(1,128)S(1)}, f32[2,1]{0,1:T(1,128)}, u32[]{:S(2)}) copy-start(f32[2,1]{0,1:T(1,128)} %param.28) | copy-start | bytes 28
  8.8 26.2 %copy-start.15 = (bf16[256,32]{0,1:T(8,128)(2,1)S(1)}, bf16[256,32]{0,1:T(8,128)(2,1)}, u32[]{:S(2)}) copy-start(bf16[256,32]{0,1:T(8,128)(2,1)} %param.29) | copy-start | bytes 49156
  21.1 128.8 %all-gather.15.cloned.1.call-start = ((), (), s32[]{:S(2)}) async-start(), calls=%async_computation.3 | async-start | bytes 1310720 | tf_op jit(solution)/shard_map/all_gather | solution.py:41
  31.2 254.2 %all-gather.21.cloned.1.call-start = ((), (), s32[]{:S(2)}) async-start(), calls=%async_computation.8 | async-start | bytes 1622016 | tf_op jit(solution)/shard_map/all_gather | solution.py:25
  32.0 398.8 %reduce-scatter.3.cloned.1.call-start = ((), (), s32[]{:S(2)}) async-start(), calls=%async_computation.4 | async-start | bytes 2359296 | tf_op jit(solution)/shard_map/reduce_scatter | solution.py:67
  303.5 2.9 copy-start.3
  303.5 2.9 copy-start.4
  309.3 16.6 %copy-start.7 = (bf16[1024,128]{0,1:T(8,128)(2,1)S(1)}, bf16[1024,128]{0,1:T(8,128)(2,1)}, u32[]{:S(2)}) copy-start(bf16[1024,128]{0,1:T(8,128)(2,1)} %get-tuple-element.170) | copy-start | bytes 786436
  322.3 7.6 copy-start.11
  333.5 14.1 %copy-start.1 = (f32[8,256,128]{1,2,0:T(8,128)S(1)}, f32[8,256,128]{1,2,0:T(8,128)}, u32[]{:S(2)}) copy-start(f32[8,256,128]{1,2,0:T(8,128)} %fusion.105) | copy-start | bytes 3145732
  350.9 9.0 %copy-start = (f32[8,256,128]{1,2,0:T(8,128)S(1)}, f32[8,256,128]{1,2,0:T(8,128)}, u32[]{:S(2)}) copy-start(f32[8,256,128]{1,2,0:T(8,128)} %fusion.104) | copy-start | bytes 3145732
  350.9 9.0 %copy-start.6 = (bf16[1024,1,128]{2,0,1:T(8,128)(2,1)S(1)}, bf16[1024,1,128]{2,0,1:T(8,128)(2,1)}, u32[]{:S(2)}) copy-start(bf16[1024,1,128]{2,0,1:T(8,128)(2,1)} %copy.47) | copy-start | bytes 786436
  359.9 2.5 copy-start.2
  369.8 62.0 %copy-start.5 = (bf16[1,128,1024]{2,1,0:T(8,128)(2,1)S(1)}, bf16[1,128,1024]{2,1,0:T(8,128)(2,1)}, u32[]{:S(2)}) copy-start(bf16[1,128,1024]{2,1,0:T(8,128)(2,1)} %param.22) | copy-start | bytes 786436
  369.8 62.1 %copy-start.20 = (f32[1024]{0:T(1024)S(1)}, f32[1024]{0:T(1024)}, u32[]{:S(2)}) copy-start(f32[1024]{0:T(1024)} %param.30) | copy-start | bytes 12292
  369.8 63.3 %copy-start.21 = (f32[1024]{0:T(1024)S(1)}, f32[1024]{0:T(1024)}, u32[]{:S(2)}) copy-start(f32[1024]{0:T(1024)} %param.31) | copy-start | bytes 12292
  369.9 263.7 %all-gather.23.cloned.1.call-start = ((), (), s32[]{:S(2)}) async-start(), calls=%async_computation.9 | async-start | bytes 1486848 | tf_op jit(solution)/shard_map/all_gather | solution.py:25
  371.4 305.5 %all-gather.17.cloned.1.call-start = ((), (), s32[]{:S(2)}) async-start(), calls=%async_computation.5 | async-start | bytes 1572864 | tf_op jit(solution)/shard_map/all_gather | solution.py:41
  431.9 13.6 %copy-start.23 = (f32[3,352]{1,0:T(4,128)S(1)}, f32[3,352]{1,0:T(4,128)}, u32[]{:S(2)}) copy-start(f32[3,352]{1,0:T(4,128)} %param.35) | copy-start | bytes 12676
  431.9 13.5 %copy-start.24 = (f32[3,352]{1,0:T(4,128)S(1)}, f32[3,352]{1,0:T(4,128)}, u32[]{:S(2)}) copy-start(f32[3,352]{1,0:T(4,128)} %param.34) | copy-start | bytes 12676
  431.9 13.6 %copy-start.12 = (bf16[352,32]{0,1:T(8,128)(2,1)S(1)}, bf16[352,32]{0,1:T(8,128)(2,1)}, u32[]{:S(2)}) copy-start(bf16[352,32]{0,1:T(8,128)(2,1)} %param.38) | copy-start | bytes 67588
  445.4 263.0 %all-gather.19.cloned.1.call-start = ((), (), s32[]{:S(2)}) async-start(), calls=%async_computation.6 | async-start | bytes 1310720 | tf_op jit(solution)/shard_map/all_gather | solution.py:41
  660.4 99.5 %reduce-scatter.5.cloned.1.call-start = ((), (), s32[]{:S(2)}) async-start(), calls=%async_computation.7 | async-start | bytes 2359296 | tf_op jit(solution)/shard_map/reduce_scatter | solution.py:67
  708.3 1.5 copy-start.9
  709.9 1.1 copy-start.10
  711.0 1.1 copy-start.27
  717.0 44.0 %copy-start.22 = (f32[1024]{0:T(1024)S(1)}, f32[1024]{0:T(1024)}, u32[]{:S(2)}) copy-start(f32[1024]{0:T(1024)} %param.39) | copy-start | bytes 12292
  (4 other events, 3.9 us)
Sparse Core Ops, SparseCore 0:
  21.3 27.9 all-gather.12
  51.3 29.2 all-gather.14
  82.7 202.6 all-gather.20
  370.0 60.7 reduce-scatter.2
  432.7 200.7 all-gather.22
  635.5 41.3 all-gather.16
  679.0 29.2 all-gather.18
  717.1 42.7 reduce-scatter.4
where the time goes:
time: 772 us; the launch traced here: 770 us
  waiting for transfers between devices  349 us (45%)
  blocking collectives  290 us (38%)
  other arithmetic  43.3 us (6%)
  local copies, waits for them, and re-layouts  40.7 us (5%)
  matrix products  29.9 us (4%)
  between operations  15.5 us (2%)
    all_gather x2, waiting for transfers between devices, gather_together(): lines, at, gathered = (lax.all_gather(flat, axis), 0, [])  204 us
    all_gather x1, blocking collectives, per_device(): down_columns = lax.all_gather(down_weight, 'fs', axis=1, tiled=True)  117 us
    all_gather x1, blocking collectives, per_device(): output_columns = lax.all_gather(mixer_output, 'fs', axis=1, tiled=True)  114 us
    reduce_scatter x2, waiting for transfers between devices, own_rows_2(): lax.psum_scatter(everything.astype(jnp.bfloat16), axis, scatter_dimension...  102 us
    all_gather x4, blocking collectives, all_blocks(): pieces = lax.all_gather(pieces, axes[k], axis=0, tiled=True)  59.4 us
    all_gather x4, waiting for transfers between devices, all_blocks(): pieces = lax.all_gather(pieces, axes[k], axis=0, tiled=True)  42.4 us
  transfers between devices with their start and end apart: 8, of which 6 were waited for; matrix products, arithmetic and copies ran while one was open for 2% of the time, Pallas kernels for 0%

commit v1 on v0

v1 whole, which is shorter than its diff:
```python
import functools

import jax
import jax.numpy as jnp
import numpy as np
from jax import lax
from jax.experimental import pallas as pl
from jax.experimental.pallas import tpu as pltpu
from jax.sharding import PartitionSpec as P

MESH = pl.DeviceIdType.MESH
F32 = jnp.float32
BF16 = jnp.bfloat16

X, Y, Z, ZALL = 4, 4, 8, 16
D = 1024
DK = 128
DV = 256
SEQ = 1024
OWN = 128
HALF = 64
BLOCK = 256
UNIT = 32
FFP = 384
FFOWN = 352
EPS = 1e-6
NT = (((1,), (1,)), ((), ()))
TN = (((0,), (0,)), ((), ()))


def rotation_tables():
    frequency = 10000.0 ** (-np.arange(64, dtype=np.float64) / 64)

    def pair(positions):
        angles = positions[:, None] * frequency[None, :]
        cosine, sine = np.cos(angles), np.sin(angles)
        return np.concatenate([cosine, cosine], 1), np.concatenate([-sine, sine], 1)

    inner = np.concatenate(pair(np.arange(BLOCK, dtype=np.float64)), 1)
    outer = np.concatenate(pair(BLOCK * np.repeat(np.arange(X, dtype=np.float64), 8)), 1)
    return inner.astype(np.float32), outer.astype(np.float32)


def dot(a, b, dims=None):
    if dims is None:
        return jnp.dot(a, b, preferred_element_type=F32)
    return lax.dot_general(a, b, dims, preferred_element_type=F32)


def rms(values, gain):
    return values * lax.rsqrt(jnp.mean(values * values, axis=-1, keepdims=True) + EPS) * gain


def kernel(
    tok, g_in, wq, wk, wv, wg, logits, wo, g_mo, g_ci, w_gelu, w_linear, k_gelu, k_linear,
    b_gelu, b_linear, wd, g_co, inner, outer,
    out,
    xn, ch, w1, w2, wb, qs, ins, us, st, dmat, lead, tail, pf, ps, pr, rs_send, rs_recv,
    ms_send, ms_recv, up, hid, after, taps,
    ag_s, ag_r, wy_s, wy_r, wz_s, wz_r, bz_s, bz_r, by_s, by_r, pp_s, pp_r, rr_s, rr_r, mm_s, mm_r,
):
    rep, fs, tp = lax.axis_index("rep"), lax.axis_index("fs"), lax.axis_index("tp")
    x, c = tp // 2, tp % 2
    z, y = fs // Y, fs % Y
    zz = rep * Z + z

    def x_dev(step):
        return (rep, fs, lax.rem(x + step, X) * 2 + c)

    def y_dev(step):
        return (rep, z * Y + lax.rem(y + step, Y), tp)

    def z_dev(step):
        there = lax.rem(zz + step, ZALL)
        return (there // Z, lax.rem(there, Z) * Y + y, tp)

    sibling = (rep, fs, x * 2 + (1 - c))
    x_next, x_prev = x_dev(1), x_dev(X - 1)
    y_next, y_prev, y_far = y_dev(1), y_dev(Y - 1), y_dev(2)
    z_next, z_prev = z_dev(1), z_dev(ZALL - 1)

    barrier = pltpu.get_barrier_semaphore()
    for peer in (x_next, x_prev, sibling, y_next, y_prev, y_far, z_next, z_prev):
        pl.semaphore_signal(barrier, inc=1, device_id=peer, device_id_type=MESH)

    sent = []

    def send(src, dst, send_sem, recv_sem, peer):
        copy = pltpu.make_async_remote_copy(
            src_ref=src, dst_ref=dst, send_sem=send_sem, recv_sem=recv_sem,
            device_id=peer, device_id_type=MESH,
        )
        copy.start()
        sent.append(copy)

    def received(dst, send_sem, recv_sem):
        pltpu.make_async_remote_copy(
            src_ref=dst, dst_ref=dst, send_sem=send_sem, recv_sem=recv_sem,
            device_id=sibling, device_id_type=MESH,
        ).wait_recv()

    def rows(first, count):
        return pl.ds(pl.multiple_of(first, count), count)

    def ag_place(buf, d, core, half):
        chip = lax.rem(x + d, X)
        return buf.at[rows((chip * 2 + core) * OWN + half * HALF, HALF)]

    def ag_send(t, buf, k, d, half, peer):
        here = ag_place(buf, d, c, half)
        send(here, here, ag_s.at[t, k], ag_r.at[t, k], peer)

    def ag_wait(t, buf, k, d, core, half):
        received(ag_place(buf, d, core, half), ag_s.at[t, k], ag_r.at[t, k])

    def ag_start(t, buf, half):
        ag_send(t, buf, half, 0, half, x_next)
        ag_send(t, buf, 2 + half, 0, half, x_prev)
        ag_send(t, buf, 6 + half, 0, half, sibling)

    def ag_first(t, buf, half):
        ag_wait(t, buf, half, 3, c, half)
        if half == 0:
            ag_send(t, buf, 4, 3, 0, x_next)
        ag_wait(t, buf, 2 + half, 1, c, half)
        if half == 1:
            ag_send(t, buf, 5, 1, 1, x_prev)
        ag_send(t, buf, 6 + 6 + half, 3, half, sibling)
        ag_send(t, buf, 6 + 2 + half, 1, half, sibling)

    def ag_second(t, buf, half):
        ag_wait(t, buf, 4 + half, 2, c, half)
        ag_send(t, buf, 6 + 4 + half, 2, half, sibling)

    def ag_sibling(t, buf, d):
        for half in (0, 1):
            ag_wait(t, buf, 6 + 2 * d + half, d, 1 - c, half)

    def wa_y_start(t, buf):
        here = buf.at[rows(fs * UNIT, UNIT)]
        for k, peer in ((0, y_next), (1, y_prev), (2, y_far)):
            send(here, here, wy_s.at[t, k], wy_r.at[t, k], peer)

    def wa_y_wait(t, buf):
        for k, step in ((0, Y - 1), (1, 1), (2, 2)):
            there = buf.at[rows((z * Y + lax.rem(y + step, Y)) * UNIT, UNIT)]
            received(there, wy_s.at[t, k], wy_r.at[t, k])

    def wa_slab(buf, off, half):
        return buf.at[rows(lax.rem(z + off + Z, Z) * (Y * UNIT) + half * HALF, HALF)]

    def wa_z_send(t, buf, s, half, way):
        here = wa_slab(buf, -(s - 1) if way == 0 else s - 1, half)
        k = way * 8 + (s - 1) * 2 + half
        send(here, here, wz_s.at[t, k], wz_r.at[t, k], z_next if way == 0 else z_prev)

    def wa_z_wait(t, buf, s, half, way):
        k = way * 8 + (s - 1) * 2 + half
        received(wa_slab(buf, -s if way == 0 else s, half), wz_s.at[t, k], wz_r.at[t, k])

    def wa_z_start(t, buf):
        for half in (0, 1):
            for way in (0, 1):
                wa_z_send(t, buf, 1, half, way)

    def wa_z_step(t, buf, s, half):
        for way in (0, 1):
            wa_z_wait(t, buf, s, half, way)
            if s < 3 or half == way:
                wa_z_send(t, buf, s + 1, half, way)

    def wa_z_end(t, buf):
        for way in (0, 1):
            wa_z_wait(t, buf, 4, way, way)

    offsets = (0, -1, 1, -2, 2, -3, 3, 4)

    def wb_unit(off, y_at):
        return (lax.rem(z + off + Z, Z) * Y + y_at) * UNIT

    def bz_send(s, way):
        first = wb_unit(-(s - 1) if way == 0 else s - 1, y)
        if s == 4:
            here = wb.at[rows(first + way * 16, 16)]
        else:
            here = wb.at[rows(first, UNIT)]
        k = way * 4 + s - 1
        send(here, here, bz_s.at[k], bz_r.at[k], z_next if way == 0 else z_prev)

    def bz_wait(s, way):
        first = wb_unit(-s if way == 0 else s, y)
        if s == 4:
            here = wb.at[rows(first + way * 16, 16)]
        else:
            here = wb.at[rows(first, UNIT)]
        k = way * 4 + s - 1
        received(here, bz_s.at[k], bz_r.at[k])

    def by_send(j, k, y_step, peer):
        here = wb.at[rows(wb_unit(offsets[j], lax.rem(y + y_step, Y)), UNIT)]
        send(here, here, by_s.at[j, k], by_r.at[j, k], peer)

    def by_wait(j, k, y_step):
        here = wb.at[rows(wb_unit(offsets[j], lax.rem(y + y_step, Y)), UNIT)]
        received(here, by_s.at[j, k], by_r.at[j, k])

    def by_start(j):
        by_send(j, 0, 0, y_next)
        by_send(j, 1, 0, y_prev)

    def by_relay(j):
        by_wait(j, 0, 3)
        by_wait(j, 1, 1)
        if j % 2 == 0:
            by_send(j, 2, 3, y_next)
        else:
            by_send(j, 2, 1, y_prev)

    def bz_step(s):
        for way in (0, 1):
            bz_wait(s, way)
            if s < 4:
                bz_send(s + 1, way)
        if s < 4:
            by_start(2 * s - 1)
            by_start(2 * s)
        else:
            by_start(7)

    tokens = tok[...].astype(F32)
    xn[rows(tp * OWN, OWN)] = rms(tokens, g_in[...]).astype(BF16)
    own = rows(fs * UNIT, UNIT)
    w1[own, 0:128] = wq[...]
    w1[own, 128:256] = wk[...]
    w1[own, 256:512] = wv[...]
    w2[own, 0:256] = wg[...]
    eye = (
        lax.broadcasted_iota(jnp.int32, (UNIT, UNIT), 0)
        == lax.broadcasted_iota(jnp.int32, (UNIT, UNIT), 1)
    ).astype(F32).astype(BF16)
    w2[own, 256:512] = dot(eye, wo[...], NT).astype(BF16)
    wb[own] = jnp.zeros((UNIT, 3 * FFP), BF16)
    wb[own, 0:FFOWN] = w_gelu[...]
    wb[own, FFP : FFP + FFOWN] = w_linear[...]
    wb[own, 2 * FFP : 2 * FFP + FFOWN] = dot(eye, wd[...], NT).astype(BF16)

    pl.semaphore_wait(barrier, 8)

    ag_start(0, xn, 0)
    wa_y_start(0, w1)
    ag_start(0, xn, 1)
    bz_send(1, 0)
    bz_send(1, 1)
    wa_y_start(1, w2)
    by_start(0)

    log_f = -jnp.log1p(jnp.exp(-logits[0:1, 0:1]))
    log_b = -jnp.log1p(jnp.exp(-logits[1:2, 0:1]))
    at = lax.broadcasted_iota(jnp.int32, (BLOCK, BLOCK), 0)
    lane = lax.broadcasted_iota(jnp.int32, (BLOCK, BLOCK), 1)
    apart = (at - lane).astype(F32)
    dmat[...] = jnp.exp(jnp.where(at >= lane, apart * log_f, -apart * log_b))
    ahead = at.astype(F32)
    lead[...] = jnp.exp(
        jnp.where(lane < DK, (ahead + 1.0) * log_f, (float(BLOCK) - ahead) * log_b)
    )
    tail[...] = jnp.exp(jnp.where(lane < DK, (BLOCK - 1.0 - ahead) * log_f, ahead * log_b))
    step_f, step_b = jnp.exp(BLOCK * log_f), jnp.exp(BLOCK * log_b)
    taps[...] = jnp.zeros((16, FFP), F32)
    taps[0:3, 0:FFOWN] = k_gelu[...]
    taps[3:4, 0:FFOWN] = b_gelu[...]
    taps[8:11, 0:FFOWN] = k_linear[...]
    taps[11:12, 0:FFOWN] = b_linear[...]
    up[0:8] = jnp.zeros((8, 2 * FFP), F32)
    up[SEQ + 8 : SEQ + 16] = jnp.zeros((8, 2 * FFP), F32)

    wa_y_wait(0, w1)
    wa_z_start(0, w1)
    ag_first(0, xn, 0)
    wa_z_step(0, w1, 1, 0)
    wa_z_step(0, w1, 1, 1)
    ag_first(0, xn, 1)
    wa_z_step(0, w1, 2, 0)
    wa_z_step(0, w1, 2, 1)
    ag_second(0, xn, 0)
    ag_second(0, xn, 1)
    wa_z_step(0, w1, 3, 0)
    wa_z_step(0, w1, 3, 1)
    wa_y_wait(1, w2)
    wa_z_start(1, w2)
    for d in (0, 1, 3, 2):
        ag_sibling(0, xn, d)
    wa_z_end(0, w1)

    w2_tasks = [
        functools.partial(wa_z_step, 1, w2, s, half) for s in (1, 2, 3) for half in (0, 1)
    ]
    ff_tasks = [functools.partial(bz_step, s) for s in (1, 2, 3, 4)]
    ff_tasks += [functools.partial(by_relay, j) for j in range(8)]

    def pump(tasks, count):
        for _ in range(count):
            if tasks:
                tasks.pop(0)()

    for n, d in enumerate((0, 1, 3, 2)):
        i = lax.rem(x + d, X)
        here = rows(i * BLOCK, BLOCK)
        base = outer[rows(i * 8, 8)][0:1]
        base_cos, base_sin = base[:, 0:128], base[:, 128:256]
        cosine = base_cos * inner[:, 0:128] - base_sin * inner[:, 128:256]
        sine = base_sin * inner[:, 0:128] + base_cos * inner[:, 128:256]
        qk = dot(xn[here], w1[:, 0:256])
        q, k = qk[:, 0:128], qk[:, 128:256]
        q = (q * cosine + pltpu.roll(q, 64, 1) * sine).astype(BF16)
        k = ((k * cosine + pltpu.roll(k, 64, 1) * sine) * DK**-0.5).astype(BF16)
        qs[here] = q
        v = dot(xn[here], w1[:, 256:512]).astype(BF16)
        scores = (dot(q, k, NT) * dmat[...]).astype(BF16)
        ins[here] = dot(scores, v)
        kf = k.astype(F32)
        k_two = (jnp.concatenate([kf, kf], axis=1) * tail[...]).astype(BF16)
        us[here] = dot(k_two, v, TN)
        pump(w2_tasks, 1)

    total = jnp.zeros((DK, DV), F32)
    for i in range(X):
        st[i * BLOCK : i * BLOCK + DK] = total.astype(BF16)
        total = step_f * total + us[i * BLOCK : i * BLOCK + DK]
    total = jnp.zeros((DK, DV), F32)
    for i in reversed(range(X)):
        st[i * BLOCK + DK : (i + 1) * BLOCK] = total.astype(BF16)
        total = step_b * total + us[i * BLOCK + DK : (i + 1) * BLOCK]

    pump(w2_tasks, 2)
    wa_z_end(1, w2)
    pump(ff_tasks, 1)

    def rs_block(t, d, left, weights, first, width):
        for j in range(4):
            part = dot(left, weights[j * 256 : (j + 1) * 256, first : first + width], NT)
            pf[d * BLOCK : (d + 1) * BLOCK, j * 256 : (j + 1) * 256] = part
            ps[t, d * BLOCK : (d + 1) * BLOCK, j * 256 : (j + 1) * 256] = part.astype(BF16)
        send(
            ps.at[t, rows(d * BLOCK + (1 - c) * OWN, OWN)],
            pr.at[t, d], pp_s.at[t, d], pp_r.at[t, d], sibling,
        )

    def rs_pair_wait(t, d):
        received(pr.at[t, d], pp_s.at[t, d], pp_r.at[t, d])

    def rs_pair(t, d, half):
        mine = pf[rows(d * BLOCK + c * OWN + half * HALF, HALF)]
        return mine + pr[t, d, half * HALF : (half + 1) * HALF].astype(F32)

    def rs_far(t):
        rs_pair_wait(t, 2)
        for half, peer in ((0, x_next), (1, x_prev)):
            rs_send[t, half] = rs_pair(t, 2, half).astype(BF16)
            send(rs_send.at[t, half], rs_recv.at[t, half], rr_s.at[t, half], rr_r.at[t, half], peer)

    def rs_near(t, way, half, relay):
        d = 1 if way == 0 else 3
        total = rs_pair(t, d, half)
        if relay:
            received(rs_recv.at[t, half], rr_s.at[t, half], rr_r.at[t, half])
            total = total + rs_recv[t, half].astype(F32)
        k = way * 2 + half
        ms_send[t, k] = total.astype(BF16)
        peer = x_next if way == 0 else x_prev
        send(ms_send.at[t, k], ms_recv.at[t, k], mm_s.at[t, k], mm_r.at[t, k], peer)

    def rs_final(t, half):
        total = rs_pair(t, 0, half)
        for way in (0, 1):
            k = way * 2 + half
            received(ms_recv.at[t, k], mm_s.at[t, k], mm_r.at[t, k])
            total = total + ms_recv[t, k].astype(F32)
        return total

    def reduce_scatter(t, block, weights, first, width, between):
        for n, d in enumerate((2, 1, 3, 0)):
            rs_block(t, d, block(d), weights, first, width)
            if n == 1:
                rs_far(t)
            if n == 2:
                rs_pair_wait(t, 1)
                rs_near(t, 0, 1, False)
            if n == 3:
                rs_pair_wait(t, 3)
                rs_near(t, 1, 0, False)
            between(n)
        rs_near(t, 0, 0, True)
        rs_near(t, 1, 1, True)
        rs_pair_wait(t, 0)

    def mixer_block(d):
        i = lax.rem(x + d, X)
        here = rows(i * BLOCK, BLOCK)
        q = qs[here].astype(F32)
        q_two = (jnp.concatenate([q, q], axis=1) * lead[...]).astype(BF16)
        retained = ins[here] + dot(q_two, st[here])
        centred = retained - jnp.mean(retained, axis=-1, keepdims=True)
        normal = centred * lax.rsqrt(jnp.mean(centred * centred, axis=-1, keepdims=True) + EPS)
        gates = dot(xn[here], w2[:, 0:256])
        return (normal * (gates / (1.0 + jnp.exp(-gates)))).astype(BF16)

    reduce_scatter(0, mixer_block, w2, 256, 256, lambda n: pump(ff_tasks, 1))
    for half in (0, 1):
        part = slice(half * HALF, (half + 1) * HALF)
        mixed = rs_final(0, half)
        summed = (tok[part].astype(F32) + rms(mixed, g_mo[...])).astype(BF16).astype(F32)
        after[part] = summed
        ch[rows(tp * OWN + half * HALF, HALF)] = rms(summed, g_ci[...]).astype(BF16)
        ag_start(1, ch, half)

    ag_first(1, ch, 0)
    pump(ff_tasks, 4)
    ag_first(1, ch, 1)
    pump(ff_tasks, 4)
    for j in range(8):
        by_wait(j, 2, 2)
    ag_second(1, ch, 0)
    ag_second(1, ch, 1)

    for d in (0, 1, 3, 2):
        ag_sibling(1, ch, d)
        i = lax.rem(x + d, X)
        for j in range(3):
            up[pl.ds(pl.multiple_of(i * BLOCK + 8, 8), BLOCK), j * 256 : (j + 1) * 256] = dot(
                ch[rows(i * BLOCK, BLOCK)], wb[:, j * 256 : (j + 1) * 256]
            )

    def conv(first, column, at):
        near = up[pl.ds(pl.multiple_of(first, 8), 80), column : column + FFP]
        before = pltpu.roll(near, 1, 0)[8:72]
        behind = pltpu.roll(near, 79, 0)[8:72]
        return (
            taps[at : at + 1] * before
            + taps[at + 1 : at + 2] * near[8:72]
            + taps[at + 2 : at + 3] * behind
            + taps[at + 3 : at + 4]
        )

    def channel_block(d):
        i = lax.rem(x + d, X)

        def tile(n, carry):
            first = i * BLOCK + n * HALF
            g = conv(first, 0, 0)
            act = 0.5 * g * (1.0 + jnp.tanh(0.7978845608028654 * (g + 0.044715 * g * g * g)))
            hid[pl.ds(pl.multiple_of(n * HALF, HALF), HALF)] = (
                act * conv(first, FFP, 8)
            ).astype(BF16)
            return carry

        lax.fori_loop(0, BLOCK // HALF, tile, 0)
        return hid[...]

    reduce_scatter(1, channel_block, wb, 2 * FFP, FFP, lambda n: None)
    for half in (0, 1):
        part = slice(half * HALF, (half + 1) * HALF)
        out[part] = (after[part] + rms(rs_final(1, half), g_co[...])).astype(BF16)

    for copy in sent:
        copy.wait_send()


def layer(
    tokens, mixer_in_gain, query_weight, key_weight, value_weight, gate_weight, decay_logits,
    mixer_output, mixer_out_gain, channel_in_gain, gelu_weight, linear_weight, gelu_kernel,
    linear_kernel, gelu_bias, linear_bias, down_weight, channel_out_gain,
):
    inner, outer = rotation_tables()

    def row(v):
        return v.reshape(1, -1)

    operands = (
        tokens[0], row(mixer_in_gain), query_weight, key_weight, value_weight, gate_weight,
        decay_logits, mixer_output, row(mixer_out_gain), row(channel_in_gain), gelu_weight,
        linear_weight, gelu_kernel, linear_kernel, row(gelu_bias), row(linear_bias), down_weight,
        row(channel_out_gain), jnp.asarray(inner), jnp.asarray(outer),
    )
    dma = pltpu.SemaphoreType.DMA
    result = pl.pallas_call(
        kernel,
        out_shape=jax.ShapeDtypeStruct((OWN, D), BF16),
        in_specs=[pl.BlockSpec(memory_space=pltpu.VMEM)] * len(operands),
        out_specs=pl.BlockSpec(memory_space=pltpu.VMEM),
        scratch_shapes=[
            pltpu.VMEM((SEQ, D), BF16),
            pltpu.VMEM((SEQ, D), BF16),
            pltpu.VMEM((D, 512), BF16),
            pltpu.VMEM((D, 512), BF16),
            pltpu.VMEM((D, 3 * FFP), BF16),
            pltpu.VMEM((SEQ, DK), BF16),
            pltpu.VMEM((SEQ, DV), F32),
            pltpu.VMEM((SEQ, DV), F32),
            pltpu.VMEM((SEQ, DV), BF16),
            pltpu.VMEM((BLOCK, BLOCK), F32),
            pltpu.VMEM((BLOCK, BLOCK), F32),
            pltpu.VMEM((BLOCK, BLOCK), F32),
            pltpu.VMEM((SEQ, D), F32),
            pltpu.VMEM((2, SEQ, D), BF16),
            pltpu.VMEM((2, 4, OWN, D), BF16),
            pltpu.VMEM((2, 2, HALF, D), BF16),
            pltpu.VMEM((2, 2, HALF, D), BF16),
            pltpu.VMEM((2, 4, HALF, D), BF16),
            pltpu.VMEM((2, 4, HALF, D), BF16),
            pltpu.VMEM((SEQ + 16, 2 * FFP), F32),
            pltpu.VMEM((BLOCK, FFP), BF16),
            pltpu.VMEM((OWN, D), F32),
            pltpu.VMEM((16, FFP), F32),
            dma((2, 14)), dma((2, 14)),
            dma((2, 3)), dma((2, 3)),
            dma((2, 16)), dma((2, 16)),
            dma((8,)), dma((8,)),
            dma((8, 3)), dma((8, 3)),
            dma((2, 4)), dma((2, 4)),
            dma((2, 2)), dma((2, 2)),
            dma((2, 4)), dma((2, 4)),
        ],
        compiler_params=pltpu.CompilerParams(
            collective_id=0, has_side_effects=True, vmem_limit_bytes=60 * 1024 * 1024
        ),
        name="layer",
    )(*operands)
    return result[None]


def solution(mesh):
    by_position = P(("rep", "fs"), "tp", None)
    up_rows, down_rows = P("fs", "tp"), P("tp", "fs")
    in_specs = (
        by_position, P(), up_rows, up_rows, up_rows, up_rows, P(None, "tp"), down_rows, P(), P(),
        up_rows, up_rows, P(None, "tp"), P(None, "tp"), P("tp"), P("tp"), down_rows, P(),
    )
    return jax.shard_map(
        layer, mesh=mesh, in_specs=in_specs, out_specs=by_position, check_vma=False
    )
```

time: 772 us -> 106 us (0.14)
  waiting for transfers between devices: 349 us -> 0 us
  blocking collectives: 290 us -> 0 us
  Pallas kernels: 0 us -> 99.2 us
  other arithmetic: 43.3 us -> 0 us
  local copies, waits for them, and re-layouts: 40.7 us -> 6.95 us
  matrix products: 29.9 us -> 0 us
  between operations: 15.5 us -> 0.01 us
    all_gather x6 -> x0, blocking collectives: 290 us -> none  [the longest x1 117 us: per_device(): down_columns = lax.all_gather(down_weight, 'fs', axis=1, tiled=True)]
    all_gather x6 -> x0, waiting for transfers between devices: 247 us -> none  [the longest x2 204 us: gather_together(): lines, at, gathered = (lax.all_gather(flat, axis), 0, [])]
    reduce_scatter x2 -> x0, waiting for transfers between devices: 102 us -> none  [own_rows_2(): lax.psum_scatter(everything.astype(jnp.bfloat16), axis, scatter_dimension...]
    pallas_call x0 -> x1, Pallas kernels: none -> 99.2 us  [layer(): pl.pallas_call(kernel, out_shape=jax.ShapeDtypeStruct((OWN, D), BF16), in...]
    dot_general x15 -> x0, matrix products: 29.9 us -> none  [the longest x2 5.76 us: one_direction(): jnp.einsum('nchd,nhde->nche', query_blocks.astype(jnp.float32) * lead_dec...]
    another operation x13 -> x0, local copies, waits for them, and re-layouts: 19.4 us -> none
    add x16 -> x0, other arithmetic: 15.1 us -> none  [advance(): return (step_decay[:, None, None] * carried + update, carried)]
    dynamic_update_slice x16 -> x0, other arithmetic: 10.6 us -> none  [one_direction(): lax.scan(advance, jnp.zeros(updates.shape[1:], jnp.float32), updates)]
  transfers between devices with their start and end apart: 8 -> 0, of which waited for: 6 -> 0; matrix products, arithmetic and copies ran while one was open for 2% -> 0% of each run, Pallas kernels for 0% -> 0%
where the time goes in v1:
time: 106 us
  Pallas kernels  99.2 us (94%)
  local copies, waits for them, and re-layouts  6.95 us (7%)
    pallas_call x1, Pallas kernels, layer(): pl.pallas_call(kernel, out_shape=jax.ShapeDtypeStruct((OWN, D), BF16), in...  99.2 us
    unnamed x8, local copies, waits for them, and re-layouts  4.48 us
    reshape x2, local copies, waits for them, and re-layouts, row(): return v.reshape(1, -1)  2.47 us

profile of v1, /device:TPU:1, one launch (start us, length us, event | category | flops | bytes accessed | tf_op | source)
XLA Modules:
  0.0 106.1 jit_solution(11401925290734553144)
XLA Ops:
  0.0 0.0 copy-start.1
  0.0 1.3 %copy.21.logits = f32[2,1]{1,0:T(2,128)} copy(f32[2,1]{0,1:T(1,128)} %param.26) | data formatting | bytes 16 | tf_op args[6]
  1.3 1.2 %reshape.21.b_gelu = f32[1,352]{1,0:T(1,128)} reshape(f32[352]{0:T(512)} %param.34) | data formatting | bytes 2816 | tf_op jit(solution)/shard_map/reshape | solution.py:477
  2.6 1.2 %reshape.22.b_linear = f32[1,352]{1,0:T(1,128)} reshape(f32[352]{0:T(512)} %param.35) | data formatting | bytes 2816 | tf_op jit(solution)/shard_map/reshape | solution.py:477
  3.8 0.0 copy-done.1
  3.8 0.0 copy-start
  3.8 0.7 copy.22.wo
  4.5 0.0 copy-done
  4.5 0.7 copy.23.wd
  5.3 99.2 %layer.1 = bf16[128,1024]{1,0:T(8,128)(2,1)} custom-call(bf16[128,1024]{1,0:T(8,128)(2,1)} %bitcast.7, f32[1,1024]{1,0:T(1,128)} %bitcast.8, bf16[32,128]{1,0:T(8,128)(2,1)} %wq.1, bf16[32,128]{1,0:T(8,128)(2,1)} %wk.1, bf16[32,256]{1,0:T(8,128)(2,1)} %wv.1, bf16[32,256]{1,0:T(8,128)(2,1)} %wg.1, f32[2,1]{1,0:T(2,128)} %copy.21.logits, ...), custom_call_target="tpu_custom_call" | custom-call | tf_op jit(solution)/shard_map/layer/pallas_call | solution.py:486
  104.5 1.7 %copy.25 = bf16[1,128,1024]{2,1,0:T(8,128)(2,1)} copy(bf16[1,128,1024]{2,1,0:T(8,128)(2,1)} %bitcast.6) | data formatting | bytes 524288
Async XLA Ops:
  0.0 3.8 %copy-start.1 = (bf16[256,32]{0,1:T(8,128)(2,1)S(1)}, bf16[256,32]{0,1:T(8,128)(2,1)}, u32[]{:S(2)}) copy-start(bf16[256,32]{0,1:T(8,128)(2,1)} %param.27) | copy-start | bytes 49156
  3.8 0.7 copy-start

commit v2 on v1

v2 whole, which is shorter than its diff:
```python
import jax
import jax.numpy as jnp
import numpy as np
from jax import lax
from jax.experimental import pallas as pl
from jax.experimental.pallas import tpu as pltpu
from jax.sharding import PartitionSpec as P

MESH = pl.DeviceIdType.MESH
F32 = jnp.float32
BF16 = jnp.bfloat16

X, Y, Z, ZALL = 4, 4, 8, 16
D = 1024
DK = 128
DV = 256
SEQ = 1024
OWN = 128
HALF = 64
PIECE = 32
BLOCK = 256
UNIT = 32
FFP = 384
FFOWN = 352
EPS = 1e-6
NT = (((1,), (1,)), ((), ()))
TN = (((0,), (0,)), ((), ()))


def rotation_tables():
    frequency = 10000.0 ** (-np.arange(64, dtype=np.float64) / 64)

    def pair(positions):
        angles = positions[:, None] * frequency[None, :]
        cosine, sine = np.cos(angles), np.sin(angles)
        return np.concatenate([cosine, cosine], 1), np.concatenate([-sine, sine], 1)

    inner = np.concatenate(pair(np.arange(BLOCK, dtype=np.float64)), 1)
    outer = np.concatenate(pair(BLOCK * np.repeat(np.arange(X, dtype=np.float64), 8)), 1)
    return inner.astype(np.float32), outer.astype(np.float32)


def dot(a, b, dims=None):
    if dims is None:
        return jnp.dot(a, b, preferred_element_type=F32)
    return lax.dot_general(a, b, dims, preferred_element_type=F32)


def rms(values, gain):
    return values * lax.rsqrt(jnp.mean(values * values, axis=-1, keepdims=True) + EPS) * gain


def kernel(
    h_tok, h_g_in, h_wq, h_wk, h_wv, h_wg, h_logits, h_wo, h_g_mo, h_g_ci, h_gelu, h_linear,
    h_k_gelu, h_k_linear, h_b_gelu, h_b_linear, h_wd, h_g_co, h_inner, h_outer,
    out,
    tok, g_in, logits, g_mo, g_ci, k_gelu, k_linear, bias_g, bias_l, g_co, inner, outer,
    s_u, s_l, s_d,
    xn, ch, b_q, b_g, b_u, b_kv, b_o, b_ld, qs, ins, us, st, dmat, lead, tail, pf, ps, pr, rs_send, rs_recv,
    ms_send, ms_recv, up, hid, after, taps,
    in_s, ag_s, ag_r, ay_s, ay_r, az_s, az_r, bz_s, bz_r, by_s, by_r, fz_s, fz_r, pp_s, pp_r, rr_s, rr_r, mm_s, mm_r,
):
    rep, fs, tp = lax.axis_index("rep"), lax.axis_index("fs"), lax.axis_index("tp")
    x, c = tp // 2, tp % 2
    z, y = fs // Y, fs % Y
    zz = rep * Z + z

    def x_dev(step):
        return (rep, fs, lax.rem(x + step, X) * 2 + c)

    def y_dev(step):
        return (rep, z * Y + lax.rem(y + step, Y), tp)

    def z_dev(step):
        there = lax.rem(zz + step, ZALL)
        return (there // Z, lax.rem(there, Z) * Y + y, tp)

    sibling = (rep, fs, x * 2 + (1 - c))
    x_next, x_prev = x_dev(1), x_dev(X - 1)
    y_next, y_prev, y_far = y_dev(1), y_dev(Y - 1), y_dev(2)
    z_next, z_prev = z_dev(1), z_dev(ZALL - 1)
    z_two = (z_dev(2), z_dev(ZALL - 2))

    barrier = pltpu.get_barrier_semaphore()
    for peer in (x_next, x_prev, sibling, y_next, y_prev, y_far, z_next, z_prev, *z_two):
        pl.semaphore_signal(barrier, inc=1, device_id=peer, device_id_type=MESH)

    def rows(first, count):
        return pl.ds(pl.multiple_of(first, count), count)

    own = rows(fs * UNIT, UNIT)
    loads = [
        pltpu.make_async_copy(src, dst, in_s.at[k])
        for k, (src, dst) in enumerate((
            (h_tok, tok), (h_g_in, g_in), (h_wq, b_q.at[own]), (h_wk, b_kv.at[own, 0:128]),
            (h_wv, b_kv.at[own, 128:384]), (h_wg, b_g.at[own]), (h_wo, b_o.at[own]), (h_logits, logits),
            (h_gelu, s_u), (h_linear, s_l), (h_wd, s_d), (h_k_gelu, k_gelu), (h_k_linear, k_linear),
            (h_b_gelu, bias_g), (h_b_linear, bias_l), (h_g_mo, g_mo), (h_g_ci, g_ci), (h_g_co, g_co),
            (h_inner, inner), (h_outer, outer),
        ))
    ]
    for load in loads:
        load.start()

    sent = []

    def send(src, dst, send_sem, recv_sem, peer):
        copy = pltpu.make_async_remote_copy(
            src_ref=src, dst_ref=dst, send_sem=send_sem, recv_sem=recv_sem,
            device_id=peer, device_id_type=MESH,
        )
        copy.start()
        sent.append(copy)

    def received(dst, send_sem, recv_sem):
        pltpu.make_async_remote_copy(
            src_ref=dst, dst_ref=dst, send_sem=send_sem, recv_sem=recv_sem,
            device_id=sibling, device_id_type=MESH,
        ).wait_recv()

    def ag_place(buf, d, core, p):
        chip = lax.rem(x + d, X)
        return buf.at[rows((chip * 2 + core) * OWN + p * PIECE, PIECE)]

    def ag_send(t, buf, k, d, p, peer):
        here = ag_place(buf, d, c, p)
        send(here, here, ag_s.at[t, k], ag_r.at[t, k], peer)

    def ag_wait(t, buf, k, d, core, p):
        received(ag_place(buf, d, core, p), ag_s.at[t, k], ag_r.at[t, k])

    def ag_start(t, buf, *pieces):
        for p in pieces:
            ag_send(t, buf, p, 0, p, x_next)
            ag_send(t, buf, 4 + p, 0, p, x_prev)
            ag_send(t, buf, 12 + p, 0, p, sibling)

    def ag_first(t, buf, *pieces):
        for p in pieces:
            ag_wait(t, buf, p, 3, c, p)
            if p < 2:
                ag_send(t, buf, 8 + p, 3, p, x_next)
            ag_send(t, buf, 24 + p, 3, p, sibling)
            ag_wait(t, buf, 4 + p, 1, c, p)
            if p >= 2:
                ag_send(t, buf, 8 + p, 1, p, x_prev)
            ag_send(t, buf, 16 + p, 1, p, sibling)

    def ag_second(t, buf, *pieces):
        for p in pieces:
            ag_wait(t, buf, 8 + p, 2, c, p)
            ag_send(t, buf, 20 + p, 2, p, sibling)

    def ag_sibling(t, buf, d):
        for p in range(4):
            ag_wait(t, buf, 12 + 4 * d + p, d, 1 - c, p)

    class FastZ:
        def hop(self, off, k, peer, piece=None):
            here = self.piece(off, piece)
            send(here, here, fz_s.at[self.f, k], fz_r.at[self.f, k], peer)

        def landed(self, off, k, piece=None):
            received(self.piece(off, piece), fz_s.at[self.f, k], fz_r.at[self.f, k])

        def fast_start(self):
            for way, one, two in ((0, z_next, z_two[0]), (1, z_prev, z_two[1])):
                self.hop(0, way * 4 + 1, two)
                self.hop(0, way * 4, one)

        def fast_one(self):
            self.landed(-1, 0)
            self.landed(1, 4)

        def fast_relay(self):
            self.landed(-2, 1)
            self.hop(-2, 3, z_two[0], 0)
            self.hop(-2, 2, z_next)
            self.landed(2, 5)
            self.hop(2, 7, z_two[1], 1)
            self.hop(2, 6, z_prev)

        def fast_end(self):
            self.landed(-3, 2)
            self.landed(3, 6)
            self.landed(4, 3, 0)
            self.landed(4, 7, 1)

    class OverYZ(FastZ):
        def __init__(self, n, buf, f=None):
            self.n, self.buf, self.f = n, buf, f

        def piece(self, off, half):
            first = lax.rem(z + off + Z, Z) * (Y * UNIT)
            if half is None:
                return self.buf.at[rows(first, Y * UNIT)]
            return self.buf.at[rows(first + half * HALF, HALF)]

        def y_start(self):
            here = self.buf.at[rows(fs * UNIT, UNIT)]
            for k, peer in ((0, y_next), (1, y_prev), (2, y_far)):
                send(here, here, ay_s.at[self.n, k], ay_r.at[self.n, k], peer)

        def y_wait(self):
            for k, step in ((0, Y - 1), (1, 1), (2, 2)):
                there = self.buf.at[rows((z * Y + lax.rem(y + step, Y)) * UNIT, UNIT)]
                received(there, ay_s.at[self.n, k], ay_r.at[self.n, k])

        def slab(self, off, half):
            first = lax.rem(z + off + Z, Z) * (Y * UNIT) + half * HALF
            return self.buf.at[rows(first, HALF)]

        def z_send(self, s, half, way):
            here = self.slab(-(s - 1) if way == 0 else s - 1, half)
            k = way * 8 + (s - 1) * 2 + half
            peer = z_next if way == 0 else z_prev
            send(here, here, az_s.at[self.n, k], az_r.at[self.n, k], peer)

        def z_wait(self, s, half, way):
            k = way * 8 + (s - 1) * 2 + half
            there = self.slab(-s if way == 0 else s, half)
            received(there, az_s.at[self.n, k], az_r.at[self.n, k])

        def z_start(self):
            self.y_wait()
            for half in (0, 1):
                for way in (0, 1):
                    self.z_send(1, half, way)

        def z_step(self, s):
            for half in (0, 1):
                for way in (0, 1):
                    self.z_wait(s, half, way)
                    if s < 3 or half == way:
                        self.z_send(s + 1, half, way)

        def z_end(self):
            for way in (0, 1):
                self.z_wait(4, way, way)

    offsets = (0, -1, 1, -2, 2, -3, 3, 4)

    class OverZY(FastZ):
        def __init__(self, n, buf, f=None):
            self.n, self.buf, self.f = n, buf, f

        def piece(self, off, half):
            first = self.unit(off, 0)
            if half is None:
                return self.buf.at[rows(first, UNIT)]
            return self.buf.at[rows(first + half * 16, 16)]

        def unit(self, off, y_step):
            return (lax.rem(z + off + Z, Z) * Y + lax.rem(y + y_step, Y)) * UNIT

        def z_part(self, off, s, way):
            if s == 4:
                return self.buf.at[rows(self.unit(off, 0) + way * 16, 16)]
            return self.buf.at[rows(self.unit(off, 0), UNIT)]

        def z_send(self, s, way):
            here = self.z_part(-(s - 1) if way == 0 else s - 1, s, way)
            k = way * 4 + s - 1
            peer = z_next if way == 0 else z_prev
            send(here, here, bz_s.at[self.n, k], bz_r.at[self.n, k], peer)

        def z_start(self):
            self.z_send(1, 0)
            self.z_send(1, 1)

        def z_step(self, s):
            for way in (0, 1):
                there = self.z_part(-s if way == 0 else s, s, way)
                received(there, bz_s.at[self.n, way * 4 + s - 1], bz_r.at[self.n, way * 4 + s - 1])
                if s < 4:
                    self.z_send(s + 1, way)
            self.y_start(*((2 * s - 1, 2 * s) if s < 4 else (7,)))

        def y_send(self, j, k, y_step, peer):
            here = self.buf.at[rows(self.unit(offsets[j], y_step), UNIT)]
            send(here, here, by_s.at[self.n, j, k], by_r.at[self.n, j, k], peer)

        def y_wait(self, j, k, y_step):
            there = self.buf.at[rows(self.unit(offsets[j], y_step), UNIT)]
            received(there, by_s.at[self.n, j, k], by_r.at[self.n, j, k])

        def y_start(self, *slots):
            for j in slots:
                self.y_send(j, 0, 0, y_next)
                self.y_send(j, 1, 0, y_prev)

        def y_relay(self, *slots):
            for j in slots:
                if j % 2 == 0:
                    self.y_wait(j, 0, 3)
                    self.y_send(j, 2, 3, y_next)
                    self.y_wait(j, 1, 1)
                else:
                    self.y_wait(j, 1, 1)
                    self.y_send(j, 2, 1, y_prev)
                    self.y_wait(j, 0, 3)

        def y_end(self, *slots):
            for j in slots:
                self.y_wait(j, 2, 2)

    w_q, w_g, w_u = OverYZ(0, b_q, 0), OverYZ(1, b_g), OverYZ(2, b_u)
    w_kv, w_o, w_ld = OverZY(0, b_kv, 1), OverZY(1, b_o, 2), OverZY(2, b_ld)

    for k in (0, 1, 2, 3, 4, 5, 6, 7):
        loads[k].wait()
    tokens = tok[...].astype(F32)
    xn[rows(tp * OWN, OWN)] = rms(tokens, g_in[...]).astype(BF16)
    for k in range(8, len(loads)):
        loads[k].wait()
    b_u[own] = jnp.zeros((UNIT, FFP), BF16)
    b_u[own, 0:FFOWN] = s_u[...]
    b_ld[own] = jnp.zeros((UNIT, 2 * FFP), BF16)
    b_ld[own, 0:FFOWN] = s_l[...]
    b_ld[own, FFP : FFP + FFOWN] = s_d[...]

    pl.semaphore_wait(barrier, 10)

    ag_start(0, xn, 0, 2)
    w_q.y_start()
    w_kv.fast_start()
    w_kv.y_start(0)
    ag_start(0, xn, 1, 3)
    w_o.fast_start()
    w_g.y_start()

    log_f = -jnp.log1p(jnp.exp(-logits[0:1, 0:1]))
    log_b = -jnp.log1p(jnp.exp(-logits[0:1, 1:2]))
    at = lax.broadcasted_iota(jnp.int32, (BLOCK, BLOCK), 0)
    lane = lax.broadcasted_iota(jnp.int32, (BLOCK, BLOCK), 1)
    apart = (at - lane).astype(F32)
    dmat[...] = jnp.exp(jnp.where(at >= lane, apart * log_f, -apart * log_b))
    ahead = at.astype(F32)
    lead[...] = jnp.exp(
        jnp.where(lane < DK, (ahead + 1.0) * log_f, (float(BLOCK) - ahead) * log_b)
    )
    tail[...] = jnp.exp(jnp.where(lane < DK, (BLOCK - 1.0 - ahead) * log_f, ahead * log_b))
    step_f, step_b = jnp.exp(BLOCK * log_f), jnp.exp(BLOCK * log_b)
    taps[...] = jnp.zeros((16, FFP), F32)
    taps[0:3, 0:FFOWN] = k_gelu[...]
    taps[3:4, 0:FFOWN] = bias_g[...].reshape(1, FFOWN)
    taps[8:11, 0:FFOWN] = k_linear[...]
    taps[11:12, 0:FFOWN] = bias_l[...].reshape(1, FFOWN)
    up[0:8] = jnp.zeros((8, 2 * FFP), F32)
    up[SEQ + 8 : SEQ + 16] = jnp.zeros((8, 2 * FFP), F32)

    w_q.y_wait()
    w_q.fast_start()
    w_kv.fast_one()
    w_kv.fast_relay()
    w_kv.y_start(1, 2, 3, 4)
    ag_first(0, xn, 0, 2)
    w_o.fast_one()
    w_o.fast_relay()
    w_g.z_start()
    w_kv.y_relay(0)
    w_o.y_start(0, 1, 2)
    ag_first(0, xn, 1, 3)
    w_q.fast_relay()
    w_kv.y_relay(1, 2, 3, 4)
    w_kv.fast_end()
    w_kv.y_start(5, 6, 7)
    w_g.z_step(1)
    w_o.y_start(3, 4)
    w_o.fast_end()
    w_o.y_start(5, 6, 7)
    w_ld.z_start()
    w_u.y_start()
    w_ld.y_start(0)
    ag_second(0, xn, 0, 2, 1, 3)
    ag_sibling(0, xn, 0)
    ag_sibling(0, xn, 1)
    ag_sibling(0, xn, 3)
    w_q.fast_one()
    w_q.fast_end()
    w_kv.y_relay(5, 6, 7)
    w_o.y_relay(0, 1, 2, 3, 4)
    w_g.z_step(2)
    ag_sibling(0, xn, 2)
    w_kv.y_end(*range(8))

    def between_qkv(n):
        if n == 0:
            w_ld.z_step(1)
        elif n == 1:
            w_o.y_relay(5, 6, 7)
        elif n == 2:
            w_g.z_step(3)
        else:
            w_u.z_start()
            w_ld.y_relay(0)

    def between_mixer(n):
        if n == 0:
            w_ld.z_step(2)
        elif n == 1:
            w_ld.y_relay(1, 2)
        elif n == 2:
            w_u.z_step(1)
        else:
            w_ld.z_step(3)

    for n, d in enumerate((0, 1, 3, 2)):
        i = lax.rem(x + d, X)
        here = rows(i * BLOCK, BLOCK)
        base = outer[rows(i * 8, 8)][0:1]
        base_cos, base_sin = base[:, 0:128], base[:, 128:256]
        cosine = base_cos * inner[:, 0:128] - base_sin * inner[:, 128:256]
        sine = base_sin * inner[:, 0:128] + base_cos * inner[:, 128:256]
        q = dot(xn[here], b_q[...])
        kv = dot(xn[here], b_kv[...])
        k = kv[:, 0:128]
        q = (q * cosine + pltpu.roll(q, 64, 1) * sine).astype(BF16)
        k = ((k * cosine + pltpu.roll(k, 64, 1) * sine) * DK**-0.5).astype(BF16)
        qs[here] = q
        v = kv[:, 128:384].astype(BF16)
        scores = (dot(q, k, NT) * dmat[...]).astype(BF16)
        ins[here] = dot(scores, v)
        kf = k.astype(F32)
        k_two = (jnp.concatenate([kf, kf], axis=1) * tail[...]).astype(BF16)
        us[here] = dot(k_two, v, TN)
        between_qkv(n)

    total = jnp.zeros((DK, DV), F32)
    for i in range(X):
        st[i * BLOCK : i * BLOCK + DK] = total.astype(BF16)
        total = step_f * total + us[i * BLOCK : i * BLOCK + DK]
    total = jnp.zeros((DK, DV), F32)
    for i in reversed(range(X)):
        st[i * BLOCK + DK : (i + 1) * BLOCK] = total.astype(BF16)
        total = step_b * total + us[i * BLOCK + DK : (i + 1) * BLOCK]

    w_g.z_end()
    w_o.y_end(*range(8))

    def rs_block(t, d, left, weights, first, width):
        for j in range(4):
            part = dot(left, weights[j * 256 : (j + 1) * 256, first : first + width], NT)
            pf[d * BLOCK : (d + 1) * BLOCK, j * 256 : (j + 1) * 256] = part
            ps[t, d * BLOCK : (d + 1) * BLOCK, j * 256 : (j + 1) * 256] = part.astype(BF16)
        send(
            ps.at[t, rows(d * BLOCK + (1 - c) * OWN, OWN)],
            pr.at[t, d], pp_s.at[t, d], pp_r.at[t, d], sibling,
        )

    def rs_pair_wait(t, d):
        received(pr.at[t, d], pp_s.at[t, d], pp_r.at[t, d])

    def rs_pair(t, d, p):
        mine = pf[rows(d * BLOCK + c * OWN + p * PIECE, PIECE)]
        return mine + pr[t, d, p * PIECE : (p + 1) * PIECE].astype(F32)

    def rs_far(t):
        rs_pair_wait(t, 2)
        for p in (0, 2, 1, 3):
            rs_send[t, p] = rs_pair(t, 2, p).astype(BF16)
            peer = x_next if p < 2 else x_prev
            send(rs_send.at[t, p], rs_recv.at[t, p], rr_s.at[t, p], rr_r.at[t, p], peer)

    def rs_near(t, way, p, relay):
        total = rs_pair(t, 1 if way == 0 else 3, p)
        if relay:
            received(rs_recv.at[t, p], rr_s.at[t, p], rr_r.at[t, p])
            total = total + rs_recv[t, p].astype(F32)
        k = way * 4 + p
        ms_send[t, k] = total.astype(BF16)
        peer = x_next if way == 0 else x_prev
        send(ms_send.at[t, k], ms_recv.at[t, k], mm_s.at[t, k], mm_r.at[t, k], peer)

    def rs_final(t, p):
        total = rs_pair(t, 0, p)
        for k in (p, 4 + p):
            received(ms_recv.at[t, k], mm_s.at[t, k], mm_r.at[t, k])
            total = total + ms_recv[t, k].astype(F32)
        return total

    def reduce_scatter(t, block, weights, first, width, between):
        for n, d in enumerate((2, 1, 3, 0)):
            rs_block(t, d, block(d), weights, first, width)
            if n == 1:
                rs_far(t)
            if n == 2:
                rs_pair_wait(t, 1)
                rs_near(t, 0, 2, False)
                rs_near(t, 0, 3, False)
            if n == 3:
                rs_pair_wait(t, 3)
                rs_near(t, 1, 0, False)
                rs_near(t, 1, 1, False)
            between(n)
        for p in (0, 2, 1, 3):
            rs_near(t, 0 if p < 2 else 1, p, True)
        rs_pair_wait(t, 0)

    def mixer_block(d):
        i = lax.rem(x + d, X)
        here = rows(i * BLOCK, BLOCK)
        q = qs[here].astype(F32)
        q_two = (jnp.concatenate([q, q], axis=1) * lead[...]).astype(BF16)
        retained = ins[here] + dot(q_two, st[here])
        centred = retained - jnp.mean(retained, axis=-1, keepdims=True)
        normal = centred * lax.rsqrt(jnp.mean(centred * centred, axis=-1, keepdims=True) + EPS)
        gates = dot(xn[here], b_g[...])
        return (normal * (gates / (1.0 + jnp.exp(-gates)))).astype(BF16)

    reduce_scatter(0, mixer_block, b_o, 0, 256, between_mixer)
    for p in (0, 2, 1, 3):
        part = slice(p * PIECE, (p + 1) * PIECE)
        mixed = rs_final(0, p)
        summed = (tok[part].astype(F32) + rms(mixed, g_mo[...])).astype(BF16).astype(F32)
        after[part] = summed
        ch[rows(tp * OWN + p * PIECE, PIECE)] = rms(summed, g_ci[...]).astype(BF16)
        ag_start(1, ch, p)

    w_ld.z_step(4)
    w_u.z_step(2)
    w_ld.y_relay(3, 4)
    ag_first(1, ch, 0, 2)
    w_ld.y_relay(5, 6)
    w_u.z_step(3)
    w_ld.y_relay(7)
    ag_first(1, ch, 1, 3)
    w_u.z_end()
    w_ld.y_end(*range(8))
    ag_second(1, ch, 0, 2, 1, 3)

    for d in (0, 1, 3, 2):
        ag_sibling(1, ch, d)
        i = lax.rem(x + d, X)
        there = pl.ds(pl.multiple_of(i * BLOCK + 8, 8), BLOCK)
        up[there, 0:FFP] = dot(ch[rows(i * BLOCK, BLOCK)], b_u[...])
        up[there, FFP:] = dot(ch[rows(i * BLOCK, BLOCK)], b_ld[:, 0:FFP])

    def conv(first, column, at):
        near = up[pl.ds(pl.multiple_of(first, 8), 80), column : column + FFP]
        before = pltpu.roll(near, 1, 0)[8:72]
        behind = pltpu.roll(near, 79, 0)[8:72]
        return (
            taps[at : at + 1] * before
            + taps[at + 1 : at + 2] * near[8:72]
            + taps[at + 2 : at + 3] * behind
            + taps[at + 3 : at + 4]
        )

    def channel_block(d):
        i = lax.rem(x + d, X)

        def tile(n, carry):
            first = i * BLOCK + n * HALF
            g = conv(first, 0, 0)
            act = 0.5 * g * (1.0 + jnp.tanh(0.7978845608028654 * (g + 0.044715 * g * g * g)))
            hid[pl.ds(pl.multiple_of(n * HALF, HALF), HALF)] = (
                act * conv(first, FFP, 8)
            ).astype(BF16)
            return carry

        lax.fori_loop(0, BLOCK // HALF, tile, 0)
        return hid[...]

    reduce_scatter(1, channel_block, b_ld, FFP, FFP, lambda n: None)
    for p in (0, 2, 1, 3):
        part = slice(p * PIECE, (p + 1) * PIECE)
        out[part] = (after[part] + rms(rs_final(1, p), g_co[...])).astype(BF16)

    for copy in sent:
        copy.wait_send()


def layer(
    tokens, mixer_in_gain, query_weight, key_weight, value_weight, gate_weight, decay_logits,
    mixer_output, mixer_out_gain, channel_in_gain, gelu_weight, linear_weight, gelu_kernel,
    linear_kernel, gelu_bias, linear_bias, down_weight, channel_out_gain,
):
    inner, outer = rotation_tables()

    def row(v):
        return v.reshape(1, -1)

    operands = (
        tokens[0], row(mixer_in_gain), query_weight, key_weight, value_weight, gate_weight,
        decay_logits.T, mixer_output.T, row(mixer_out_gain), row(channel_in_gain), gelu_weight,
        linear_weight, gelu_kernel, linear_kernel, gelu_bias, linear_bias, down_weight.T,
        row(channel_out_gain), jnp.asarray(inner), jnp.asarray(outer),
    )
    dma = pltpu.SemaphoreType.DMA
    result = pl.pallas_call(
        kernel,
        out_shape=jax.ShapeDtypeStruct((OWN, D), BF16),
        in_specs=[pl.BlockSpec(memory_space=pl.ANY)] * len(operands),
        out_specs=pl.BlockSpec(memory_space=pltpu.VMEM),
        scratch_shapes=[
            pltpu.VMEM((OWN, D), BF16),
            pltpu.VMEM((1, D), F32),
            pltpu.VMEM((1, 2), F32),
            pltpu.VMEM((1, D), F32),
            pltpu.VMEM((1, D), F32),
            pltpu.VMEM((3, FFOWN), F32),
            pltpu.VMEM((3, FFOWN), F32),
            pltpu.VMEM((FFOWN,), F32),
            pltpu.VMEM((FFOWN,), F32),
            pltpu.VMEM((1, D), F32),
            pltpu.VMEM((BLOCK, 256), F32),
            pltpu.VMEM((8 * X, 256), F32),
            pltpu.VMEM((UNIT, FFOWN), BF16),
            pltpu.VMEM((UNIT, FFOWN), BF16),
            pltpu.VMEM((UNIT, FFOWN), BF16),
            pltpu.VMEM((SEQ, D), BF16),
            pltpu.VMEM((SEQ, D), BF16),
            pltpu.VMEM((D, 128), BF16),
            pltpu.VMEM((D, 256), BF16),
            pltpu.VMEM((D, FFP), BF16),
            pltpu.VMEM((D, 384), BF16),
            pltpu.VMEM((D, 256), BF16),
            pltpu.VMEM((D, 2 * FFP), BF16),
            pltpu.VMEM((SEQ, DK), BF16),
            pltpu.VMEM((SEQ, DV), F32),
            pltpu.VMEM((SEQ, DV), F32),
            pltpu.VMEM((SEQ, DV), BF16),
            pltpu.VMEM((BLOCK, BLOCK), F32),
            pltpu.VMEM((BLOCK, BLOCK), F32),
            pltpu.VMEM((BLOCK, BLOCK), F32),
            pltpu.VMEM((SEQ, D), F32),
            pltpu.VMEM((2, SEQ, D), BF16),
            pltpu.VMEM((2, 4, OWN, D), BF16),
            pltpu.VMEM((2, 4, PIECE, D), BF16),
            pltpu.VMEM((2, 4, PIECE, D), BF16),
            pltpu.VMEM((2, 8, PIECE, D), BF16),
            pltpu.VMEM((2, 8, PIECE, D), BF16),
            pltpu.VMEM((SEQ + 16, 2 * FFP), F32),
            pltpu.VMEM((BLOCK, FFP), BF16),
            pltpu.VMEM((OWN, D), F32),
            pltpu.VMEM((16, FFP), F32),
            dma((20,)),
            dma((2, 28)), dma((2, 28)),
            dma((3, 3)), dma((3, 3)),
            dma((3, 16)), dma((3, 16)),
            dma((3, 8)), dma((3, 8)),
            dma((3, 8, 3)), dma((3, 8, 3)),
            dma((3, 8)), dma((3, 8)),
            dma((2, 4)), dma((2, 4)),
            dma((2, 4)), dma((2, 4)),
            dma((2, 8)), dma((2, 8)),
        ],
        compiler_params=pltpu.CompilerParams(
            collective_id=0, has_side_effects=True, vmem_limit_bytes=60 * 1024 * 1024
        ),
        name="layer",
    )(*operands)
    return result[None]


def solution(mesh):
    by_position = P(("rep", "fs"), "tp", None)
    up_rows, down_rows = P("fs", "tp"), P("tp", "fs")
    in_specs = (
        by_position, P(), up_rows, up_rows, up_rows, up_rows, P(None, "tp"), down_rows, P(), P(),
        up_rows, up_rows, P(None, "tp"), P(None, "tp"), P("tp"), P("tp"), down_rows, P(),
    )
    return jax.shard_map(
        layer, mesh=mesh, in_specs=in_specs, out_specs=by_position, check_vma=False
    )
```

time: 106 us -> 86.2 us (0.81)
  Pallas kernels: 99.2 us -> 84.4 us
  local copies, waits for them, and re-layouts: 6.95 us -> 1.67 us
    pallas_call x1, Pallas kernels: 99.2 us -> 84.4 us  [layer(): pl.pallas_call(kernel, out_shape=jax.ShapeDtypeStruct((OWN, D), BF16), in...]
    unnamed x8 -> x1, local copies, waits for them, and re-layouts: 4.48 us -> 1.67 us
    reshape x2 -> x0, local copies, waits for them, and re-layouts: 2.47 us -> none  [row(): return v.reshape(1, -1)]
where the time goes in v2:
time: 86.2 us; the launch traced here: 86 us
  Pallas kernels  84.4 us (98%)
  local copies, waits for them, and re-layouts  1.67 us (2%)
    pallas_call x1, Pallas kernels, layer(): pl.pallas_call(kernel, out_shape=jax.ShapeDtypeStruct((OWN, D), BF16), in...  84.4 us

profile of v2, /device:TPU:1, one launch (start us, length us, event | category | flops | bytes accessed | tf_op | source)
XLA Modules:
  0.0 86.0 jit_solution(14010746553048158716)
XLA Ops:
  0.0 84.4 %layer.1 = bf16[128,1024]{1,0:T(8,128)(2,1)} custom-call(bf16[128,1024]{1,0:T(8,128)(2,1)} %bitcast.10, f32[1,1024]{1,0:T(1,128)} %bitcast.13, bf16[32,128]{1,0:T(8,128)(2,1)} %h_wq.1, bf16[32,128]{1,0:T(8,128)(2,1)} %h_wk.1, bf16[32,256]{1,0:T(8,128)(2,1)} %h_wv.1, bf16[32,256]{1,0:T(8,128)(2,1)} %h_wg.1, f32[1,2]{1,0:T(1,128)} %bitcast.17, ...), custom_call_target="tpu_custom_call" | custom-call | tf_op jit(solution)/shard_map/layer/pallas_call | solution.py:591
  84.4 1.7 %copy.22 = bf16[1,128,1024]{2,1,0:T(8,128)(2,1)} copy(bf16[1,128,1024]{2,1,0:T(8,128)(2,1)} %bitcast.9) | data formatting | bytes 524288

commit v3 on v2

--- a/solution.py
+++ b/solution.py
@@ -56,9 +56,9 @@
     out,
     tok, g_in, logits, g_mo, g_ci, k_gelu, k_linear, bias_g, bias_l, g_co, inner, outer,
     s_u, s_l, s_d,
-    xn, ch, b_q, b_g, b_u, b_kv, b_o, b_ld, qs, ins, us, st, dmat, lead, tail, pf, ps, pr, rs_send, rs_recv,
+    xn, ch, b_k, b_g, b_u, b_v, b_qo, b_ld, ks, vs, us, st, dmat, lead, tail, pf, ps, pr, rs_send, rs_recv,
     ms_send, ms_recv, up, hid, after, taps,
-    in_s, ag_s, ag_r, ay_s, ay_r, az_s, az_r, bz_s, bz_r, by_s, by_r, fz_s, fz_r, pp_s, pp_r, rr_s, rr_r, mm_s, mm_r,
+    in_s, ag_s, ag_r, ay_s, ay_r, by_s, by_r, fz_s, fz_r, pp_s, pp_r, rr_s, rr_r, mm_s, mm_r,
 ):
     rep, fs, tp = lax.axis_index("rep"), lax.axis_index("fs"), lax.axis_index("tp")
     x, c = tp // 2, tp % 2
@@ -92,8 +92,8 @@
     loads = [
         pltpu.make_async_copy(src, dst, in_s.at[k])
         for k, (src, dst) in enumerate((
-            (h_tok, tok), (h_g_in, g_in), (h_wq, b_q.at[own]), (h_wk, b_kv.at[own, 0:128]),
-            (h_wv, b_kv.at[own, 128:384]), (h_wg, b_g.at[own]), (h_wo, b_o.at[own]), (h_logits, logits),
+            (h_tok, tok), (h_g_in, g_in), (h_wq, b_qo.at[own, 0:128]), (h_wk, b_k.at[own]),
+            (h_wv, b_v.at[own]), (h_wg, b_g.at[own]), (h_wo, b_qo.at[own, 128:384]), (h_logits, logits),
             (h_gelu, s_u), (h_linear, s_l), (h_wd, s_d), (h_k_gelu, k_gelu), (h_k_linear, k_linear),
             (h_b_gelu, bias_g), (h_b_linear, bias_l), (h_g_mo, g_mo), (h_g_ci, g_ci), (h_g_co, g_co),
             (h_inner, inner), (h_outer, outer),
@@ -163,10 +163,17 @@
         def landed(self, off, k, piece=None):
             received(self.piece(off, piece), fz_s.at[self.f, k], fz_r.at[self.f, k])
 
+        def start_two(self):
+            self.hop(0, 1, z_two[0])
+            self.hop(0, 5, z_two[1])
+
+        def start_one(self):
+            self.hop(0, 0, z_next)
+            self.hop(0, 4, z_prev)
+
         def fast_start(self):
-            for way, one, two in ((0, z_next, z_two[0]), (1, z_prev, z_two[1])):
-                self.hop(0, way * 4 + 1, two)
-                self.hop(0, way * 4, one)
+            self.start_two()
+            self.start_one()
 
         def fast_one(self):
             self.landed(-1, 0)
@@ -206,38 +213,6 @@
                 there = self.buf.at[rows((z * Y + lax.rem(y + step, Y)) * UNIT, UNIT)]
                 received(there, ay_s.at[self.n, k], ay_r.at[self.n, k])
 
-        def slab(self, off, half):
-            first = lax.rem(z + off + Z, Z) * (Y * UNIT) + half * HALF
-            return self.buf.at[rows(first, HALF)]
-
-        def z_send(self, s, half, way):
-            here = self.slab(-(s - 1) if way == 0 else s - 1, half)
-            k = way * 8 + (s - 1) * 2 + half
-            peer = z_next if way == 0 else z_prev
-            send(here, here, az_s.at[self.n, k], az_r.at[self.n, k], peer)
-
-        def z_wait(self, s, half, way):
-            k = way * 8 + (s - 1) * 2 + half
-            there = self.slab(-s if way == 0 else s, half)
-            received(there, az_s.at[self.n, k], az_r.at[self.n, k])
-
-        def z_start(self):
-            self.y_wait()
-            for half in (0, 1):
-                for way in (0, 1):
-                    self.z_send(1, half, way)
-
-        def z_step(self, s):
-            for half in (0, 1):
-                for way in (0, 1):
-                    self.z_wait(s, half, way)
-                    if s < 3 or half == way:
-                        self.z_send(s + 1, half, way)
-
-        def z_end(self):
-            for way in (0, 1):
-                self.z_wait(4, way, way)
-
     offsets = (0, -1, 1, -2, 2, -3, 3, 4)
 
     class OverZY(FastZ):
@@ -252,29 +227,6 @@
 
         def unit(self, off, y_step):
             return (lax.rem(z + off + Z, Z) * Y + lax.rem(y + y_step, Y)) * UNIT
-
-        def z_part(self, off, s, way):
-            if s == 4:
-                return self.buf.at[rows(self.unit(off, 0) + way * 16, 16)]
-            return self.buf.at[rows(self.unit(off, 0), UNIT)]
-
-        def z_send(self, s, way):
-            here = self.z_part(-(s - 1) if way == 0 else s - 1, s, way)
-            k = way * 4 + s - 1
-            peer = z_next if way == 0 else z_prev
-            send(here, here, bz_s.at[self.n, k], bz_r.at[self.n, k], peer)
-
-        def z_start(self):
-            self.z_send(1, 0)
-            self.z_send(1, 1)
-
-        def z_step(self, s):
-            for way in (0, 1):
-                there = self.z_part(-s if way == 0 else s, s, way)
-                received(there, bz_s.at[self.n, way * 4 + s - 1], bz_r.at[self.n, way * 4 + s - 1])
-                if s < 4:
-                    self.z_send(s + 1, way)
-            self.y_start(*((2 * s - 1, 2 * s) if s < 4 else (7,)))
 
         def y_send(self, j, k, y_step, peer):
             here = self.buf.at[rows(self.unit(offsets[j], y_step), UNIT)]
@@ -304,8 +256,8 @@
             for j in slots:
                 self.y_wait(j, 2, 2)
 
-    w_q, w_g, w_u = OverYZ(0, b_q, 0), OverYZ(1, b_g), OverYZ(2, b_u)
-    w_kv, w_o, w_ld = OverZY(0, b_kv, 1), OverZY(1, b_o, 2), OverZY(2, b_ld)
+    w_k, w_g, w_u = OverYZ(0, b_k, 0), OverYZ(1, b_g, 1), OverYZ(2, b_u, 2)
+    w_v, w_qo, w_ld = OverZY(0, b_v, 3), OverZY(1, b_qo, 4), OverZY(2, b_ld, 5)
 
     for k in (0, 1, 2, 3, 4, 5, 6, 7):
         loads[k].wait()
@@ -322,12 +274,13 @@
     pl.semaphore_wait(barrier, 10)
 
     ag_start(0, xn, 0, 2)
-    w_q.y_start()
-    w_kv.fast_start()
-    w_kv.y_start(0)
+    w_v.fast_start()
+    w_k.y_start()
+    w_v.y_start(0)
     ag_start(0, xn, 1, 3)
-    w_o.fast_start()
+    w_qo.fast_start()
     w_g.y_start()
+    w_qo.y_start(0)
 
     log_f = -jnp.log1p(jnp.exp(-logits[0:1, 0:1]))
     log_b = -jnp.log1p(jnp.exp(-logits[0:1, 1:2]))
@@ -349,82 +302,75 @@
     up[0:8] = jnp.zeros((8, 2 * FFP), F32)
     up[SEQ + 8 : SEQ + 16] = jnp.zeros((8, 2 * FFP), F32)
 
-    w_q.y_wait()
-    w_q.fast_start()
-    w_kv.fast_one()
-    w_kv.fast_relay()
-    w_kv.y_start(1, 2, 3, 4)
+    w_v.fast_relay()
+    w_v.fast_one()
+    w_v.y_start(1, 2, 3, 4)
+    w_k.y_wait()
+    w_k.fast_start()
     ag_first(0, xn, 0, 2)
-    w_o.fast_one()
-    w_o.fast_relay()
-    w_g.z_start()
-    w_kv.y_relay(0)
-    w_o.y_start(0, 1, 2)
+    w_qo.fast_relay()
+    w_qo.fast_one()
+    w_qo.y_start(1, 2, 3, 4)
+    w_g.y_wait()
+    w_g.start_two()
+    w_v.y_relay(0)
     ag_first(0, xn, 1, 3)
-    w_q.fast_relay()
-    w_kv.y_relay(1, 2, 3, 4)
-    w_kv.fast_end()
-    w_kv.y_start(5, 6, 7)
-    w_g.z_step(1)
-    w_o.y_start(3, 4)
-    w_o.fast_end()
-    w_o.y_start(5, 6, 7)
-    w_ld.z_start()
-    w_u.y_start()
-    w_ld.y_start(0)
-    ag_second(0, xn, 0, 2, 1, 3)
+    w_v.fast_end()
+    w_v.y_start(5, 6, 7)
+    w_v.y_relay(1, 2, 3, 4)
+    w_qo.y_relay(0)
+    w_k.fast_relay()
+    w_g.start_one()
+    w_qo.fast_end()
+    w_qo.y_start(5, 6, 7)
+    ag_second(0, xn, 0, 2)
+    w_v.y_relay(5, 6, 7)
+    ag_second(0, xn, 1, 3)
+    w_qo.y_relay(1, 2, 3, 4)
+    w_g.fast_relay()
     ag_sibling(0, xn, 0)
     ag_sibling(0, xn, 1)
     ag_sibling(0, xn, 3)
-    w_q.fast_one()
-    w_q.fast_end()
-    w_kv.y_relay(5, 6, 7)
-    w_o.y_relay(0, 1, 2, 3, 4)
-    w_g.z_step(2)
     ag_sibling(0, xn, 2)
-    w_kv.y_end(*range(8))
-
-    def between_qkv(n):
+    w_k.fast_one()
+    w_k.fast_end()
+    w_v.y_end(*range(8))
+
+    def between_keys(n):
         if n == 0:
-            w_ld.z_step(1)
-        elif n == 1:
-            w_o.y_relay(5, 6, 7)
+            w_qo.y_relay(5, 6, 7)
+            w_u.y_start()
+            w_ld.fast_start()
         elif n == 2:
-            w_g.z_step(3)
-        else:
-            w_u.z_start()
-            w_ld.y_relay(0)
+            w_ld.y_start(0)
 
     def between_mixer(n):
         if n == 0:
-            w_ld.z_step(2)
+            w_ld.fast_relay()
+            w_u.y_wait()
+            w_u.fast_start()
         elif n == 1:
-            w_ld.y_relay(1, 2)
-        elif n == 2:
-            w_u.z_step(1)
-        else:
-            w_ld.z_step(3)
-
-    for n, d in enumerate((0, 1, 3, 2)):
-        i = lax.rem(x + d, X)
-        here = rows(i * BLOCK, BLOCK)
+            w_ld.fast_one()
+            w_ld.y_start(1, 2, 3, 4)
+
+    def turn(values, i):
         base = outer[rows(i * 8, 8)][0:1]
         base_cos, base_sin = base[:, 0:128], base[:, 128:256]
         cosine = base_cos * inner[:, 0:128] - base_sin * inner[:, 128:256]
         sine = base_sin * inner[:, 0:128] + base_cos * inner[:, 128:256]
-        q = dot(xn[here], b_q[...])
-        kv = dot(xn[here], b_kv[...])
-        k = kv[:, 0:128]
-        q = (q * cosine + pltpu.roll(q, 64, 1) * sine).astype(BF16)
-        k = ((k * cosine + pltpu.roll(k, 64, 1) * sine) * DK**-0.5).astype(BF16)
-        qs[here] = q
-        v = kv[:, 128:384].astype(BF16)
-        scores = (dot(q, k, NT) * dmat[...]).astype(BF16)
-        ins[here] = dot(scores, v)
+        return values * cosine + pltpu.roll(values, 64, 1) * sine
+
+    for n, d in enumerate((0, 1, 3, 2)):
+        i = lax.rem(x + d, X)
+        here = rows(i * BLOCK, BLOCK)
+        k = (turn(dot(xn[here], b_k[...]), i) * DK**-0.5).astype(BF16)
+        v = dot(xn[here], b_v[...]).astype(BF16)
+        ks[here] = k
+        vs[here] = v
         kf = k.astype(F32)
         k_two = (jnp.concatenate([kf, kf], axis=1) * tail[...]).astype(BF16)
         us[here] = dot(k_two, v, TN)
-        between_qkv(n)
+        between_keys(n)
 
     total = jnp.zeros((DK, DV), F32)
     for i in range(X):
@@ -435,8 +381,10 @@
         st[i * BLOCK + DK : (i + 1) * BLOCK] = total.astype(BF16)
         total = step_b * total + us[i * BLOCK + DK : (i + 1) * BLOCK]
 
-    w_g.z_end()
-    w_o.y_end(*range(8))
+
+    w_g.fast_one()
+    w_g.fast_end()
+    w_qo.y_end(*range(8))
 
     def rs_block(t, d, left, weights, first, width):
         for j in range(4):
@@ -500,41 +448,53 @@
     def mixer_block(d):
         i = lax.rem(x + d, X)
         here = rows(i * BLOCK, BLOCK)
-        q = qs[here].astype(F32)
-        q_two = (jnp.concatenate([q, q], axis=1) * lead[...]).astype(BF16)
-        retained = ins[here] + dot(q_two, st[here])
+        q = turn(dot(xn[here], b_qo[:, 0:DK]), i).astype(BF16)
+        scores = (dot(q, ks[here], NT) * dmat[...]).astype(BF16)
+        qf = q.astype(F32)
+        q_two = (jnp.concatenate([qf, qf], axis=1) * lead[...]).astype(BF16)
+        retained = dot(scores, vs[here]) + dot(q_two, st[here])
         centred = retained - jnp.mean(retained, axis=-1, keepdims=True)
         normal = centred * lax.rsqrt(jnp.mean(centred * centred, axis=-1, keepdims=True) + EPS)
         gates = dot(xn[here], b_g[...])
         return (normal * (gates / (1.0 + jnp.exp(-gates)))).astype(BF16)
 
-    reduce_scatter(0, mixer_block, b_o, 0, 256, between_mixer)
-    for p in (0, 2, 1, 3):
+    reduce_scatter(0, mixer_block, b_qo, DK, DV, between_mixer)
+    w_ld.fast_end()
+    w_ld.y_start(5, 6, 7)
+    for n, p in enumerate((0, 2, 1, 3)):
         part = slice(p * PIECE, (p + 1) * PIECE)
         mixed = rs_final(0, p)
         summed = (tok[part].astype(F32) + rms(mixed, g_mo[...])).astype(BF16).astype(F32)
         after[part] = summed
         ch[rows(tp * OWN + p * PIECE, PIECE)] = rms(summed, g_ci[...]).astype(BF16)
         ag_start(1, ch, p)
-
-    w_ld.z_step(4)
-    w_u.z_step(2)
-    w_ld.y_relay(3, 4)
+        if n == 0:
+            w_ld.y_relay(0, 1, 2)
+        elif n == 1:
+            w_u.fast_relay()
+        elif n == 2:
+            w_ld.y_relay(3, 4)
+
+    w_ld.y_relay(5, 6, 7)
     ag_first(1, ch, 0, 2)
-    w_ld.y_relay(5, 6)
-    w_u.z_step(3)
-    w_ld.y_relay(7)
     ag_first(1, ch, 1, 3)
-    w_u.z_end()
-    w_ld.y_end(*range(8))
-    ag_second(1, ch, 0, 2, 1, 3)
-
-    for d in (0, 1, 3, 2):
+
+    def expand(d):
         ag_sibling(1, ch, d)
         i = lax.rem(x + d, X)
         there = pl.ds(pl.multiple_of(i * BLOCK + 8, 8), BLOCK)
         up[there, 0:FFP] = dot(ch[rows(i * BLOCK, BLOCK)], b_u[...])
         up[there, FFP:] = dot(ch[rows(i * BLOCK, BLOCK)], b_ld[:, 0:FFP])
+
+    w_u.fast_one()
+    w_u.fast_end()
+    w_ld.y_end(*range(8))
+    expand(0)
+    ag_second(1, ch, 0, 2)
+    expand(1)
+    ag_second(1, ch, 1, 3)
+    expand(3)
+    expand(2)
 
     def conv(first, column, at):
         near = up[pl.ds(pl.multiple_of(first, 8), 80), column : column + FFP]
@@ -611,14 +571,14 @@
             pltpu.VMEM((UNIT, FFOWN), BF16),
             pltpu.VMEM((SEQ, D), BF16),
             pltpu.VMEM((SEQ, D), BF16),
-            pltpu.VMEM((D, 128), BF16),
-            pltpu.VMEM((D, 256), BF16),
+            pltpu.VMEM((D, DK), BF16),
+            pltpu.VMEM((D, DV), BF16),
             pltpu.VMEM((D, FFP), BF16),
-            pltpu.VMEM((D, 384), BF16),
-            pltpu.VMEM((D, 256), BF16),
+            pltpu.VMEM((D, DV), BF16),
+            pltpu.VMEM((D, DK + DV), BF16),
             pltpu.VMEM((D, 2 * FFP), BF16),
             pltpu.VMEM((SEQ, DK), BF16),
-            pltpu.VMEM((SEQ, DV), F32),
+            pltpu.VMEM((SEQ, DV), BF16),
             pltpu.VMEM((SEQ, DV), F32),
             pltpu.VMEM((SEQ, DV), BF16),
             pltpu.VMEM((BLOCK, BLOCK), F32),
@@ -638,10 +598,8 @@
             dma((20,)),
             dma((2, 28)), dma((2, 28)),
             dma((3, 3)), dma((3, 3)),
-            dma((3, 16)), dma((3, 16)),
-            dma((3, 8)), dma((3, 8)),
             dma((3, 8, 3)), dma((3, 8, 3)),
-            dma((3, 8)), dma((3, 8)),
+            dma((6, 8)), dma((6, 8)),
             dma((2, 4)), dma((2, 4)),
             dma((2, 4)), dma((2, 4)),
             dma((2, 8)), dma((2, 8)),

time: 86.2 us -> 80.4 us (0.933)
  Pallas kernels: 84.4 us -> 78.5 us
    pallas_call x1, Pallas kernels: 84.4 us -> 78.5 us  [layer(): pl.pallas_call(kernel, out_shape=jax.ShapeDtypeStruct((OWN, D), BF16), in...]
where the time goes in v3:
time: 80.4 us; the launch traced here: 80.2 us
  Pallas kernels  78.5 us (98%)
  local copies, waits for them, and re-layouts  1.67 us (2%)
    pallas_call x1, Pallas kernels, layer(): pl.pallas_call(kernel, out_shape=jax.ShapeDtypeStruct((OWN, D), BF16), in...  78.5 us
    unnamed x1, local copies, waits for them, and re-layouts  1.67 us

profile of v3, /device:TPU:1, one launch (start us, length us, event | category | flops | bytes accessed | tf_op | source)
XLA Modules:
  0.0 80.2 jit_solution(8219627808044186333)
XLA Ops:
  0.0 78.5 %layer.1 = bf16[128,1024]{1,0:T(8,128)(2,1)} custom-call(bf16[128,1024]{1,0:T(8,128)(2,1)} %bitcast.10, f32[1,1024]{1,0:T(1,128)} %bitcast.13, bf16[32,128]{1,0:T(8,128)(2,1)} %h_wq.1, bf16[32,128]{1,0:T(8,128)(2,1)} %h_wk.1, bf16[32,256]{1,0:T(8,128)(2,1)} %h_wv.1, bf16[32,256]{1,0:T(8,128)(2,1)} %h_wg.1, f32[1,2]{1,0:T(1,128)} %bitcast.17, ...), custom_call_target="tpu_custom_call" | custom-call | tf_op jit(solution)/shard_map/layer/pallas_call | solution.py:551
  78.5 1.7 %copy.22 = bf16[1,128,1024]{2,1,0:T(8,128)(2,1)} copy(bf16[1,128,1024]{2,1,0:T(8,128)(2,1)} %bitcast.9) | data formatting | bytes 524288

commit v4 on v3

--- a/solution.py
+++ b/solution.py
@@ -56,7 +56,7 @@
     out,
     tok, g_in, logits, g_mo, g_ci, k_gelu, k_linear, bias_g, bias_l, g_co, inner, outer,
     s_u, s_l, s_d,
-    xn, ch, b_k, b_g, b_u, b_v, b_qo, b_ld, ks, vs, us, st, dmat, lead, tail, pf, ps, pr, rs_send, rs_recv,
+    xn, ch, b_k, b_g, b_u, b_v, b_qo, b_ld, ks, vs, silu, us, st, dmat, lead, tail, pf, ps, pr, rs_send, rs_recv,
     ms_send, ms_recv, up, hid, after, taps,
     in_s, ag_s, ag_r, ay_s, ay_r, by_s, by_r, fz_s, fz_r, pp_s, pp_r, rr_s, rr_r, mm_s, mm_r,
 ):
@@ -335,21 +335,14 @@
     w_k.fast_one()
     w_k.fast_end()
     w_v.y_end(*range(8))
-
-    def between_keys(n):
-        if n == 0:
-            w_qo.y_relay(5, 6, 7)
-            w_u.y_start()
-            w_ld.fast_start()
-        elif n == 2:
-            w_ld.y_start(0)
+    w_qo.y_relay(5, 6, 7)
 
     def between_mixer(n):
-        if n == 0:
+        if n == 1:
             w_ld.fast_relay()
             w_u.y_wait()
             w_u.fast_start()
-        elif n == 1:
+        elif n == 2:
             w_ld.fast_one()
             w_ld.y_start(1, 2, 3, 4)
 
@@ -360,17 +353,23 @@
         sine = base_sin * inner[:, 0:128] + base_cos * inner[:, 128:256]
         return values * cosine + pltpu.roll(values, 64, 1) * sine
 
-    for n, d in enumerate((0, 1, 3, 2)):
-        i = lax.rem(x + d, X)
-        here = rows(i * BLOCK, BLOCK)
-        k = (turn(dot(xn[here], b_k[...]), i) * DK**-0.5).astype(BF16)
-        v = dot(xn[here], b_v[...]).astype(BF16)
-        ks[here] = k
-        vs[here] = v
-        kf = k.astype(F32)
-        k_two = (jnp.concatenate([kf, kf], axis=1) * tail[...]).astype(BF16)
-        us[here] = dot(k_two, v, TN)
-        between_keys(n)
+    for pair in range(2):
+        wide = slice(pair * 2 * BLOCK, (pair + 1) * 2 * BLOCK)
+        k_wide = dot(xn[wide], b_k[...])
+        v_wide = dot(xn[wide], b_v[...]).astype(BF16)
+        vs[wide] = v_wide
+        for n in range(2):
+            i = 2 * pair + n
+            here, inside = slice(i * BLOCK, (i + 1) * BLOCK), slice(n * BLOCK, (n + 1) * BLOCK)
+            k = (turn(k_wide[inside], i) * DK**-0.5).astype(BF16)
+            ks[here] = k
+            kf = k.astype(F32)
+            k_two = (jnp.concatenate([kf, kf], axis=1) * tail[...]).astype(BF16)
+            us[here] = dot(k_two, v_wide[inside], TN)
+        if pair == 0:
+            w_u.y_start()
+            w_ld.fast_start()
+            w_ld.y_start(0)
 
     total = jnp.zeros((DK, DV), F32)
     for i in range(X):
@@ -384,6 +383,10 @@
 
     w_g.fast_one()
     w_g.fast_end()
+    for pair in range(2):
+        wide = slice(pair * 2 * BLOCK, (pair + 1) * 2 * BLOCK)
+        gates = dot(xn[wide], b_g[...])
+        silu[wide] = gates / (1.0 + jnp.exp(-gates))
     w_qo.y_end(*range(8))
 
     def rs_block(t, d, left, weights, first, width):
@@ -391,20 +394,18 @@
             part = dot(left, weights[j * 256 : (j + 1) * 256, first : first + width], NT)
             pf[d * BLOCK : (d + 1) * BLOCK, j * 256 : (j + 1) * 256] = part
             ps[t, d * BLOCK : (d + 1) * BLOCK, j * 256 : (j + 1) * 256] = part.astype(BF16)
-        send(
-            ps.at[t, rows(d * BLOCK + (1 - c) * OWN, OWN)],
-            pr.at[t, d], pp_s.at[t, d], pp_r.at[t, d], sibling,
-        )
-
-    def rs_pair_wait(t, d):
-        received(pr.at[t, d], pp_s.at[t, d], pp_r.at[t, d])
+        for p in (0, 2, 1, 3):
+            send(
+                ps.at[t, rows(d * BLOCK + (1 - c) * OWN + p * PIECE, PIECE)],
+                pr.at[t, d, pl.ds(p * PIECE, PIECE)], pp_s.at[t, d, p], pp_r.at[t, d, p], sibling,
+            )
 
     def rs_pair(t, d, p):
+        received(pr.at[t, d, pl.ds(p * PIECE, PIECE)], pp_s.at[t, d, p], pp_r.at[t, d, p])
         mine = pf[rows(d * BLOCK + c * OWN + p * PIECE, PIECE)]
         return mine + pr[t, d, p * PIECE : (p + 1) * PIECE].astype(F32)
 
     def rs_far(t):
-        rs_pair_wait(t, 2)
         for p in (0, 2, 1, 3):
             rs_send[t, p] = rs_pair(t, 2, p).astype(BF16)
             peer = x_next if p < 2 else x_prev
@@ -433,17 +434,16 @@
             if n == 1:
                 rs_far(t)
             if n == 2:
-                rs_pair_wait(t, 1)
                 rs_near(t, 0, 2, False)
-                rs_near(t, 0, 3, False)
             if n == 3:
-                rs_pair_wait(t, 3)
                 rs_near(t, 1, 0, False)
-                rs_near(t, 1, 1, False)
             between(n)
-        for p in (0, 2, 1, 3):
-            rs_near(t, 0 if p < 2 else 1, p, True)
-        rs_pair_wait(t, 0)
+        rs_near(t, 0, 0, True)
+        rs_near(t, 1, 2, True)
+        rs_near(t, 0, 3, False)
+        rs_near(t, 1, 1, False)
+        rs_near(t, 0, 1, True)
+        rs_near(t, 1, 3, True)
 
     def mixer_block(d):
         i = lax.rem(x + d, X)
@@ -455,8 +455,7 @@
         retained = dot(scores, vs[here]) + dot(q_two, st[here])
         centred = retained - jnp.mean(retained, axis=-1, keepdims=True)
         normal = centred * lax.rsqrt(jnp.mean(centred * centred, axis=-1, keepdims=True) + EPS)
-        gates = dot(xn[here], b_g[...])
-        return (normal * (gates / (1.0 + jnp.exp(-gates)))).astype(BF16)
+        return (normal * silu[here]).astype(BF16)
 
     reduce_scatter(0, mixer_block, b_qo, DK, DV, between_mixer)
     w_ld.fast_end()
@@ -483,8 +482,10 @@
         ag_sibling(1, ch, d)
         i = lax.rem(x + d, X)
         there = pl.ds(pl.multiple_of(i * BLOCK + 8, 8), BLOCK)
-        up[there, 0:FFP] = dot(ch[rows(i * BLOCK, BLOCK)], b_u[...])
-        up[there, FFP:] = dot(ch[rows(i * BLOCK, BLOCK)], b_ld[:, 0:FFP])
+        left = ch[rows(i * BLOCK, BLOCK)]
+        up[there, 0:256] = dot(left, b_u[:, 0:256])
+        up[there, 256:512] = dot(left, jnp.concatenate([b_u[:, 256:384], b_ld[:, 0:128]], axis=1))
+        up[there, 512:768] = dot(left, b_ld[:, 128:384])
 
     w_u.fast_one()
     w_u.fast_end()
@@ -547,11 +548,12 @@
         linear_weight, gelu_kernel, linear_kernel, gelu_bias, linear_bias, down_weight.T,
         row(channel_out_gain), jnp.asarray(inner), jnp.asarray(outer),
     )
+    operands = [pltpu.with_memory_space_constraint(v, pltpu.HBM) for v in operands]
     dma = pltpu.SemaphoreType.DMA
     result = pl.pallas_call(
         kernel,
-        out_shape=jax.ShapeDtypeStruct((OWN, D), BF16),
-        in_specs=[pl.BlockSpec(memory_space=pl.ANY)] * len(operands),
+        out_shape=pltpu.VMEM((OWN, D), BF16),
+        in_specs=[pl.BlockSpec(memory_space=pltpu.HBM)] * len(operands),
         out_specs=pl.BlockSpec(memory_space=pltpu.VMEM),
         scratch_shapes=[
             pltpu.VMEM((OWN, D), BF16),
@@ -580,6 +582,7 @@
             pltpu.VMEM((SEQ, DK), BF16),
             pltpu.VMEM((SEQ, DV), BF16),
             pltpu.VMEM((SEQ, DV), F32),
+            pltpu.VMEM((SEQ, DV), F32),
             pltpu.VMEM((SEQ, DV), BF16),
             pltpu.VMEM((BLOCK, BLOCK), F32),
             pltpu.VMEM((BLOCK, BLOCK), F32),
@@ -600,12 +603,12 @@
             dma((3, 3)), dma((3, 3)),
             dma((3, 8, 3)), dma((3, 8, 3)),
             dma((6, 8)), dma((6, 8)),
-            dma((2, 4)), dma((2, 4)),
+            dma((2, 4, 4)), dma((2, 4, 4)),
             dma((2, 4)), dma((2, 4)),
             dma((2, 8)), dma((2, 8)),
         ],
         compiler_params=pltpu.CompilerParams(
-            collective_id=0, has_side_effects=True, vmem_limit_bytes=60 * 1024 * 1024
+            collective_id=0, has_side_effects=True, vmem_limit_bytes=40 * 1024 * 1024
         ),
         name="layer",
     )(*operands)

time: 80.4 us -> 77.1 us (0.959)
  Pallas kernels: 78.5 us -> 76.3 us
  local copies, waits for them, and re-layouts: 1.67 us -> 0.71 us
    pallas_call x1, Pallas kernels: 78.5 us -> 76.3 us  [layer(): pl.pallas_call(kernel, out_shape=pltpu.VMEM((OWN, D), BF16), in_specs=[pl...]
    unnamed x1, local copies, waits for them, and re-layouts: 1.67 us -> 0.71 us
where the time goes in v4:
time: 77.1 us; the launch traced here: 77 us
  Pallas kernels  76.3 us (99%)
    pallas_call x1, Pallas kernels, layer(): pl.pallas_call(kernel, out_shape=pltpu.VMEM((OWN, D), BF16), in_specs=[pl...  76.3 us

profile of v4, /device:TPU:1, one launch (start us, length us, event | category | flops | bytes accessed | tf_op | source)
XLA Modules:
  0.0 77.0 jit_solution(1331565656759562461)
XLA Ops:
  0.0 76.3 %layer.1 = bf16[128,1024]{1,0:T(8,128)(2,1)S(1)} custom-call(bf16[128,1024]{1,0:T(8,128)(2,1)} %bitcast.10, f32[1,1024]{1,0:T(1,128)} %bitcast.13, bf16[32,128]{1,0:T(8,128)(2,1)} %h_wq.1, bf16[32,128]{1,0:T(8,128)(2,1)} %h_wk.1, bf16[32,256]{1,0:T(8,128)(2,1)} %h_wv.1, bf16[32,256]{1,0:T(8,128)(2,1)} %h_wg.1, f32[1,2]{1,0:T(1,128)} %bitcast.17, ...), custom_call_target="tpu_custom_call" | custom-call | tf_op jit(solution)/shard_map/layer/pallas_call | solution.py:553
  76.3 0.7 copy.22

commit v5 on v4

--- a/solution.py
+++ b/solution.py
@@ -57,7 +57,7 @@
     tok, g_in, logits, g_mo, g_ci, k_gelu, k_linear, bias_g, bias_l, g_co, inner, outer,
     s_u, s_l, s_d,
     xn, ch, b_k, b_g, b_u, b_v, b_qo, b_ld, ks, vs, silu, us, st, dmat, lead, tail, pf, ps, pr, rs_send, rs_recv,
-    ms_send, ms_recv, up, hid, after, taps,
+    ms_send, ms_recv, up, hid, gated, after, taps,
     in_s, ag_s, ag_r, ay_s, ay_r, by_s, by_r, fz_s, fz_r, pp_s, pp_r, rr_s, rr_r, mm_s, mm_r,
 ):
     rep, fs, tp = lax.axis_index("rep"), lax.axis_index("fs"), lax.axis_index("tp")
@@ -104,13 +104,37 @@
 
     sent = []
 
+    def drain(count):
+        for copy in sent[:count]:
+            copy.wait_send()
+        del sent[:count]
+
+
+    held = [None]
+
     def send(src, dst, send_sem, recv_sem, peer):
         copy = pltpu.make_async_remote_copy(
             src_ref=src, dst_ref=dst, send_sem=send_sem, recv_sem=recv_sem,
             device_id=peer, device_id_type=MESH,
         )
-        copy.start()
         sent.append(copy)
+        if held[0] is None:
+            copy.start()
+        else:
+            held[0].append(copy)
+
+    def prepare(*sends):
+        held[0] = []
+        for one in sends:
+            one()
+        copies, held[0] = held[0], None
+        return copies
+
+    def start_on(core, copies):
+        @pl.when(c == core)
+        def _():
+            for copy in copies:
+                copy.start()
 
     def received(dst, send_sem, recv_sem):
         pltpu.make_async_remote_copy(
@@ -310,7 +334,8 @@
     ag_first(0, xn, 0, 2)
     w_qo.fast_relay()
     w_qo.fast_one()
-    w_qo.y_start(1, 2, 3, 4)
+    qo_y = prepare(lambda: w_qo.y_start(1, 2, 3, 4))
+    start_on(0, qo_y)
     w_g.y_wait()
     w_g.start_two()
     w_v.y_relay(0)
@@ -318,6 +343,7 @@
     w_v.fast_end()
     w_v.y_start(5, 6, 7)
     w_v.y_relay(1, 2, 3, 4)
+    start_on(1, qo_y)
     w_qo.y_relay(0)
     w_k.fast_relay()
     w_g.start_one()
@@ -389,20 +415,25 @@
         silu[wide] = gates / (1.0 + jnp.exp(-gates))
     w_qo.y_end(*range(8))
 
+    first_sends = len(sent)
+
     def rs_block(t, d, left, weights, first, width):
+        left = jnp.concatenate([left[rows((1 - c) * OWN, OWN)], left[rows(c * OWN, OWN)]], axis=0)
+        there = slice(d * OWN, (d + 1) * OWN)
         for j in range(4):
-            part = dot(left, weights[j * 256 : (j + 1) * 256, first : first + width], NT)
-            pf[d * BLOCK : (d + 1) * BLOCK, j * 256 : (j + 1) * 256] = part
-            ps[t, d * BLOCK : (d + 1) * BLOCK, j * 256 : (j + 1) * 256] = part.astype(BF16)
+            columns = slice(j * 256, (j + 1) * 256)
+            part = dot(left, weights[columns, first : first + width], NT)
+            ps[t, there, columns] = part[:OWN].astype(BF16)
+            pf[there, columns] = part[OWN:]
         for p in (0, 2, 1, 3):
             send(
-                ps.at[t, rows(d * BLOCK + (1 - c) * OWN + p * PIECE, PIECE)],
+                ps.at[t, pl.ds(d * OWN + p * PIECE, PIECE)],
                 pr.at[t, d, pl.ds(p * PIECE, PIECE)], pp_s.at[t, d, p], pp_r.at[t, d, p], sibling,
             )
 
     def rs_pair(t, d, p):
         received(pr.at[t, d, pl.ds(p * PIECE, PIECE)], pp_s.at[t, d, p], pp_r.at[t, d, p])
-        mine = pf[rows(d * BLOCK + c * OWN + p * PIECE, PIECE)]
+        mine = pf[d * OWN + p * PIECE : d * OWN + (p + 1) * PIECE]
         return mine + pr[t, d, p * PIECE : (p + 1) * PIECE].astype(F32)
 
     def rs_far(t):
@@ -455,7 +486,8 @@
         retained = dot(scores, vs[here]) + dot(q_two, st[here])
         centred = retained - jnp.mean(retained, axis=-1, keepdims=True)
         normal = centred * lax.rsqrt(jnp.mean(centred * centred, axis=-1, keepdims=True) + EPS)
-        return (normal * silu[here]).astype(BF16)
+        gated[...] = (normal * silu[here]).astype(BF16)
+        return gated
 
     reduce_scatter(0, mixer_block, b_qo, DK, DV, between_mixer)
     w_ld.fast_end()
@@ -475,6 +507,8 @@
             w_ld.y_relay(3, 4)
 
     w_ld.y_relay(5, 6, 7)
+    drain(first_sends)
+    before_last = len(sent)
     ag_first(1, ch, 0, 2)
     ag_first(1, ch, 1, 3)
 
@@ -521,9 +555,10 @@
             return carry
 
         lax.fori_loop(0, BLOCK // HALF, tile, 0)
-        return hid[...]
+        return hid
 
     reduce_scatter(1, channel_block, b_ld, FFP, FFP, lambda n: None)
+    drain(before_last)
     for p in (0, 2, 1, 3):
         part = slice(p * PIECE, (p + 1) * PIECE)
         out[part] = (after[part] + rms(rs_final(1, p), g_co[...])).astype(BF16)
@@ -587,8 +622,8 @@
             pltpu.VMEM((BLOCK, BLOCK), F32),
             pltpu.VMEM((BLOCK, BLOCK), F32),
             pltpu.VMEM((BLOCK, BLOCK), F32),
-            pltpu.VMEM((SEQ, D), F32),
-            pltpu.VMEM((2, SEQ, D), BF16),
+            pltpu.VMEM((4 * OWN, D), F32),
+            pltpu.VMEM((2, 4 * OWN, D), BF16),
             pltpu.VMEM((2, 4, OWN, D), BF16),
             pltpu.VMEM((2, 4, PIECE, D), BF16),
             pltpu.VMEM((2, 4, PIECE, D), BF16),
@@ -596,6 +631,7 @@
             pltpu.VMEM((2, 8, PIECE, D), BF16),
             pltpu.VMEM((SEQ + 16, 2 * FFP), F32),
             pltpu.VMEM((BLOCK, FFP), BF16),
+            pltpu.VMEM((BLOCK, DV), BF16),
             pltpu.VMEM((OWN, D), F32),
             pltpu.VMEM((16, FFP), F32),
             dma((20,)),

time: 77.1 us -> 76.8 us (level)
  no operation moved by 1% of the time
where the time goes in v5:
time: 76.8 us; the launch traced here: 76.7 us
  Pallas kernels  75.9 us (99%)
    pallas_call x1, Pallas kernels, layer(): pl.pallas_call(kernel, out_shape=pltpu.VMEM((OWN, D), BF16), in_specs=[pl...  75.9 us

profile of v5, /device:TPU:1, one launch (start us, length us, event | category | flops | bytes accessed | tf_op | source)
XLA Modules:
  0.0 76.7 jit_solution(17801677186949721212)
XLA Ops:
  0.0 75.9 %layer.1 = bf16[128,1024]{1,0:T(8,128)(2,1)S(1)} custom-call(bf16[128,1024]{1,0:T(8,128)(2,1)} %bitcast.10, f32[1,1024]{1,0:T(1,128)} %bitcast.13, bf16[32,128]{1,0:T(8,128)(2,1)} %h_wq.1, bf16[32,128]{1,0:T(8,128)(2,1)} %h_wk.1, bf16[32,256]{1,0:T(8,128)(2,1)} %h_wv.1, bf16[32,256]{1,0:T(8,128)(2,1)} %h_wg.1, f32[1,2]{1,0:T(1,128)} %bitcast.17, ...), custom_call_target="tpu_custom_call" | custom-call | tf_op jit(solution)/shard_map/layer/pallas_call | solution.py:588
  75.9 0.7 copy.22

commit v6 on v5

--- a/solution.py
+++ b/solution.py
@@ -348,9 +348,12 @@
     w_k.fast_relay()
     w_g.start_one()
     w_qo.fast_end()
-    w_qo.y_start(5, 6, 7)
+    qo_late = prepare(lambda: w_qo.y_start(5, 6))
+    start_on(0, qo_late)
     ag_second(0, xn, 0, 2)
     w_v.y_relay(5, 6, 7)
+    start_on(1, qo_late)
+    w_qo.y_start(7)
     ag_second(0, xn, 1, 3)
     w_qo.y_relay(1, 2, 3, 4)
     w_g.fast_relay()
@@ -512,11 +515,11 @@
     ag_first(1, ch, 0, 2)
     ag_first(1, ch, 1, 3)
 
-    def expand(d):
-        ag_sibling(1, ch, d)
-        i = lax.rem(x + d, X)
-        there = pl.ds(pl.multiple_of(i * BLOCK + 8, 8), BLOCK)
-        left = ch[rows(i * BLOCK, BLOCK)]
+    def expand(d, core=None):
+        count = BLOCK if core is None else OWN
+        first = lax.rem(x + d, X) * BLOCK + (0 if core is None else core * OWN)
+        there = pl.ds(pl.multiple_of(first + 8, 8), count)
+        left = ch[rows(first, count)]
         up[there, 0:256] = dot(left, b_u[:, 0:256])
         up[there, 256:512] = dot(left, jnp.concatenate([b_u[:, 256:384], b_ld[:, 0:128]], axis=1))
         up[there, 512:768] = dot(left, b_ld[:, 128:384])
@@ -524,12 +527,17 @@
     w_u.fast_one()
     w_u.fast_end()
     w_ld.y_end(*range(8))
+    ag_sibling(1, ch, 0)
     expand(0)
     ag_second(1, ch, 0, 2)
+    ag_sibling(1, ch, 1)
     expand(1)
     ag_second(1, ch, 1, 3)
+    ag_sibling(1, ch, 3)
     expand(3)
-    expand(2)
+    expand(2, c)
+    ag_sibling(1, ch, 2)
+    expand(2, 1 - c)
 
     def conv(first, column, at):
         near = up[pl.ds(pl.multiple_of(first, 8), 80), column : column + FFP]

time: 76.8 us -> 76.5 us (level)
  no operation moved by 1% of the time
where the time goes in v6:
time: 76.5 us; the launch traced here: 76.4 us
  Pallas kernels  75.7 us (99%)
    pallas_call x1, Pallas kernels, layer(): pl.pallas_call(kernel, out_shape=pltpu.VMEM((OWN, D), BF16), in_specs=[pl...  75.7 us

profile of v6, /device:TPU:1, one launch (start us, length us, event | category | flops | bytes accessed | tf_op | source)
XLA Modules:
  0.0 76.4 jit_solution(12815042735035319805)
XLA Ops:
  0.0 75.7 %layer.1 = bf16[128,1024]{1,0:T(8,128)(2,1)S(1)} custom-call(bf16[128,1024]{1,0:T(8,128)(2,1)} %bitcast.10, f32[1,1024]{1,0:T(1,128)} %bitcast.13, bf16[32,128]{1,0:T(8,128)(2,1)} %h_wq.1, bf16[32,128]{1,0:T(8,128)(2,1)} %h_wk.1, bf16[32,256]{1,0:T(8,128)(2,1)} %h_wv.1, bf16[32,256]{1,0:T(8,128)(2,1)} %h_wg.1, f32[1,2]{1,0:T(1,128)} %bitcast.17, ...), custom_call_target="tpu_custom_call" | custom-call | tf_op jit(solution)/shard_map/layer/pallas_call | solution.py:596
  75.7 0.7 copy.22

commit v7 on v6

--- a/solution.py
+++ b/solution.py
@@ -339,9 +339,9 @@
     w_g.y_wait()
     w_g.start_two()
     w_v.y_relay(0)
-    ag_first(0, xn, 1, 3)
     w_v.fast_end()
     w_v.y_start(5, 6, 7)
+    ag_first(0, xn, 1, 3)
     w_v.y_relay(1, 2, 3, 4)
     start_on(1, qo_y)
     w_qo.y_relay(0)

time: 76.5 us -> 76.4 us (level)
  no operation moved by 1% of the time
where the time goes in v7:
time: 76.4 us; the launch traced here: 76.2 us
  Pallas kernels  75.5 us (99%)
    pallas_call x1, Pallas kernels, layer(): pl.pallas_call(kernel, out_shape=pltpu.VMEM((OWN, D), BF16), in_specs=[pl...  75.5 us

profile of v7, /device:TPU:1, one launch (start us, length us, event | category | flops | bytes accessed | tf_op | source)
XLA Modules:
  0.0 76.2 jit_solution(4857367282406814751)
XLA Ops:
  0.0 75.5 %layer.1 = bf16[128,1024]{1,0:T(8,128)(2,1)S(1)} custom-call(bf16[128,1024]{1,0:T(8,128)(2,1)} %bitcast.10, f32[1,1024]{1,0:T(1,128)} %bitcast.13, bf16[32,128]{1,0:T(8,128)(2,1)} %h_wq.1, bf16[32,128]{1,0:T(8,128)(2,1)} %h_wk.1, bf16[32,256]{1,0:T(8,128)(2,1)} %h_wv.1, bf16[32,256]{1,0:T(8,128)(2,1)} %h_wg.1, f32[1,2]{1,0:T(1,128)} %bitcast.17, ...), custom_call_target="tpu_custom_call" | custom-call | tf_op jit(solution)/shard_map/layer/pallas_call | solution.py:596
  75.5 0.7 copy.22

commit v8 on v7

--- a/solution.py
+++ b/solution.py
@@ -493,8 +493,6 @@
         return gated
 
     reduce_scatter(0, mixer_block, b_qo, DK, DV, between_mixer)
-    w_ld.fast_end()
-    w_ld.y_start(5, 6, 7)
     for n, p in enumerate((0, 2, 1, 3)):
         part = slice(p * PIECE, (p + 1) * PIECE)
         mixed = rs_final(0, p)
@@ -503,6 +501,8 @@
         ch[rows(tp * OWN + p * PIECE, PIECE)] = rms(summed, g_ci[...]).astype(BF16)
         ag_start(1, ch, p)
         if n == 0:
+            w_ld.fast_end()
+            w_ld.y_start(5, 6, 7)
             w_ld.y_relay(0, 1, 2)
         elif n == 1:
             w_u.fast_relay()

time: 76.4 us -> 76.9 us (level)
  no operation moved by 1% of the time
where the time goes in v8:
time: 76.9 us; the launch traced here: 76.8 us
  Pallas kernels  76.1 us (99%)
    pallas_call x1, Pallas kernels, layer(): pl.pallas_call(kernel, out_shape=pltpu.VMEM((OWN, D), BF16), in_specs=[pl...  76.1 us

profile of v8, /device:TPU:1, one launch (start us, length us, event | category | flops | bytes accessed | tf_op | source)
XLA Modules:
  0.0 76.8 jit_solution(1624150428760534872)
XLA Ops:
  0.0 76.1 %layer.1 = bf16[128,1024]{1,0:T(8,128)(2,1)S(1)} custom-call(bf16[128,1024]{1,0:T(8,128)(2,1)} %bitcast.10, f32[1,1024]{1,0:T(1,128)} %bitcast.13, bf16[32,128]{1,0:T(8,128)(2,1)} %h_wq.1, bf16[32,128]{1,0:T(8,128)(2,1)} %h_wk.1, bf16[32,256]{1,0:T(8,128)(2,1)} %h_wv.1, bf16[32,256]{1,0:T(8,128)(2,1)} %h_wg.1, f32[1,2]{1,0:T(1,128)} %bitcast.17, ...), custom_call_target="tpu_custom_call" | custom-call | tf_op jit(solution)/shard_map/layer/pallas_call | solution.py:596
  76.1 0.7 copy.22
